TPU v7x, 32 devices: a whole 2x2x4 slice. The times are simulated.
32 devices in a mesh: ep: 8 (over z, x), tp: 4 (over y, core).
Axes of the slice: x: 2, y: 2, z: 4, core: 2. Of those that a mesh axis runs over, the one named last changes fastest.
Arguments:
- mixer_input: bfloat16 [4096, 2048], P('ep'), may hold values from -5.5 to 5.5
- expert_input: bfloat16 [4096, 2048], P('ep'), may hold values from -6 to 6
- gain_mixer: float32 [2048], replicated, may hold values from 0.1 to 1.9
- gain_expert: float32 [2048], replicated, may hold values from 0.1 to 1.9
- query_weight: bfloat16 [2048, 1536], P(None, 'tp')
- key_weight: bfloat16 [2048, 256], P(None, 'tp')
- value_weight: bfloat16 [2048, 256], P(None, 'tp'), may hold values from -0.125 to 0.125
- sink_logits: float32 [24], P('tp'), may hold values from 2 to 6
- output_weight: bfloat16 [1536, 2048], P('tp'), may hold values from -0.75 to 0.75
- expert_choice: int32 [4096, 2], P('ep'), may hold values from 0 to 7, all different within a row; in each aligned block of 128 rows (0 to 127, 128 to 255, ...) at most 64 rows name the same one
- route_weights: float32 [4096, 2], P('ep'), may hold values from 0.2 to 1.2
- expert_gate: bfloat16 [8, 2048, 1024], P('ep', None, 'tp'), may hold values from -0.125 to 0.125
- expert_up: bfloat16 [8, 2048, 1024], P('ep', None, 'tp'), may hold values from -0.125 to 0.125
- expert_down: bfloat16 [8, 1024, 2048], P('ep', 'tp'), may hold values from -0.1875 to 0.1875
- shared_gate: bfloat16 [2048, 512], P(None, 'tp'), may hold values from -0.125 to 0.125
- shared_up: bfloat16 [2048, 512], P(None, 'tp'), may hold values from -0.125 to 0.125
- shared_down: bfloat16 [512, 2048], P('tp'), may hold values from -0.25 to 0.25
Outputs:
- mixer_output: bfloat16 [4096, 2048], P(('ep', 'tp'))
- expert_output: bfloat16 [4096, 2048], P(('ep', 'tp'))
Inputs may be any that keep to these rules, and one draw needn't show every extreme that they name: `expert_choice`: in each aligned block of 128 rows no expert is named by more than 64 rows, and in some block some expert is named by exactly 64 rows; the 2 entries of a row differ.
All inputs are finite; a program needn't handle non-finite values.
Results may differ from a plain program's by a relative error of at most 0.019.
Values may be sent and summed in bfloat16 or wider, within the bound.
A program may use at most 128 MiB of HBM per device.

v0:
```python
import functools

import jax
import jax.numpy as jnp
from jax import lax
from jax.experimental import pallas as pl
from jax.experimental.pallas import tpu as pltpu
from jax.sharding import PartitionSpec as P

HEAD_DIM = 64
WINDOW = 128
SEQS = 1
PIECES = 4

norm_eps = 1e-06
rope_base = 500000.0
bf16 = jnp.bfloat16
f32 = jnp.float32
MESH = pl.DeviceIdType.MESH


def frequencies(head_size):
    half_steps = jnp.arange(head_size // 2, dtype=jnp.float32)
    return rope_base ** (-(2.0 * half_steps) / head_size)


def rows_at(start, count, unit):
    return pl.ds(pl.multiple_of(start, unit), count)


def norm_into(target, source, start, count, gain):
    step = 32

    def body(i, carry):
        widened = source[rows_at(start + i * step, step, step), :].astype(f32)
        scale = lax.rsqrt(jnp.mean(widened * widened, axis=-1, keepdims=True) + norm_eps)
        target[rows_at(i * step, step, step), :] = (widened * scale * gain[...]).astype(bf16)
        return carry

    lax.fori_loop(0, count // step, body, 0)


def silu_times(gate, up):
    return gate / (1.0 + jnp.exp(-gate)) * up


def mixture_kernel(
    capacity,
    x_ref, gain_ref, choice_ref, route_ref,
    wg_ref, wu_ref, wd_ref, sg_ref, su_ref, sd_ref,
    mx_ref, mgain_ref, wq_ref, wk_ref, wv_ref, wo_ref, sink_ref, freq_ref,
    mixer_out, expert_out,
    rows_in, normed, gain, choice, route, wg, wu, wd, sg, su, sd,
    mixer_in, mixer_gain, wq, wk, wv, wo, sink, freq, queries, band, attended,
    own_rows, slots_out, slots_in, hidden, result, back, picks, weights_col,
    mixer_part, shared_part, shared_hidden, half_in, half_out, last_in,
    load_sem, far_send, far_recv, mate_send, mate_recv, pass_send, pass_recv,
    slot_send, slot_recv, back_send, back_recv, half_send, half_recv, last_send, last_recv,
    halo_send, halo_recv,
):
    ep_count = lax.axis_size("ep")
    me = lax.axis_index("ep")
    t = lax.axis_index("tp")
    parity = t % 2
    level = t // 2
    mate = t + 1 - 2 * parity
    far = (t + 2) % 4
    far_mate = (mate + 2) % 4
    tokens, width = rows_in.shape
    own = own_rows.shape[0]
    ff = wd_ref.shape[0]
    slots = slots_out.shape[0]
    piece = width // PIECES

    barrier = pltpu.get_barrier_semaphore()

    def greet(k, carry):
        pl.semaphore_signal(barrier, inc=1, device_id={"ep": (me + k) % ep_count}, device_id_type=MESH)
        return carry

    lax.fori_loop(1, ep_count, greet, 0)
    for other in (mate, far):
        pl.semaphore_signal(barrier, inc=1, device_id={"tp": other}, device_id_type=MESH)

    loads = [
        (gain_ref, gain), (choice_ref, choice), (route_ref, route), (x_ref, rows_in),
        (wg_ref, wg.at[t]), (wu_ref, wu.at[t]), (wd_ref, wd.at[rows_at(t * ff, ff, ff)]),
        (mgain_ref, mixer_gain), (freq_ref, freq), (sink_ref, sink), (mx_ref, mixer_in),
        (wq_ref, wq), (wk_ref, wk), (wv_ref, wv), (sg_ref, sg), (su_ref, su), (sd_ref, sd), (wo_ref, wo),
    ]
    loads = [pltpu.make_async_copy(a, b, load_sem.at[i]) for i, (a, b) in enumerate(loads)]
    for load in loads:
        load.start()

    pl.semaphore_wait(barrier, ep_count + 1)

    def block_views(owner):
        views = [wg.at[owner], wu.at[owner]]
        down = wd.at[rows_at(owner * ff, ff, ff)]
        return views + [down.at[:, pl.ds(c * piece, piece)] for c in range(PIECES)]

    sources = [wg_ref, wu_ref] + [wd_ref.at[:, pl.ds(c * piece, piece)] for c in range(PIECES)]

    def remote(src, dst, send, recv, device):
        return pltpu.make_async_remote_copy(
            src_ref=src, dst_ref=dst, send_sem=send, recv_sem=recv,
            device_id=device, device_id_type=MESH,
        )

    def views_copy(srcs, owner, send, recv, device):
        return [
            remote(a, b, send.at[i], recv.at[i], device)
            for i, (a, b) in enumerate(zip(srcs, block_views(owner)))
        ]

    to_far = views_copy(sources, t, far_send, far_recv, {"tp": far})
    to_mate = views_copy(sources, t, mate_send, mate_recv, {"tp": mate})
    from_far = views_copy(sources, far, far_send, far_recv, {"tp": far})
    from_mate = views_copy(sources, mate, mate_send, mate_recv, {"tp": mate})
    to_pass = views_copy(block_views(far), far, pass_send, pass_recv, {"tp": mate})
    from_pass = views_copy(block_views(far), far_mate, pass_send, pass_recv, {"tp": mate})
    for copy in to_far:
        copy.start()

    for i in (0, 1, 2, 3):
        loads[i].wait()
    norm_into(own_rows, rows_in, t * own, own, gain)
    lanes = rows_at(t * own, own, own)
    top = choice.shape[0]
    chosen = choice[:, lanes]
    row_ids = lax.broadcasted_iota(jnp.int32, (slots // capacity, own), 0)
    named = [row_ids == chosen[k : k + 1, :] for k in range(top)]
    named_any = functools.reduce(jnp.logical_or, named).astype(f32)
    earlier = lax.broadcasted_iota(jnp.int32, (own, own), 0)
    later = lax.broadcasted_iota(jnp.int32, (own, own), 1)
    ranks = jnp.dot(named_any, (earlier < later).astype(f32), preferred_element_type=f32)
    slot_rows = [
        chosen[k : k + 1, :] * capacity
        + jnp.sum(jnp.where(named[k], ranks, 0.0), axis=0, keepdims=True).astype(jnp.int32)
        for k in range(top)
    ]
    slot_ids = lax.broadcasted_iota(jnp.int32, (slots, own), 0)
    spread = functools.reduce(jnp.logical_or, [slot_ids == row for row in slot_rows])
    spread = spread.astype(f32).astype(bf16)
    for c in range(PIECES):
        cols = pl.ds(c * piece, piece)
        slots_out[:, cols] = jnp.dot(spread, own_rows[:, cols], preferred_element_type=f32).astype(bf16)

    def slot_block(ref, owner):
        return ref.at[rows_at(owner * capacity, capacity, capacity)]

    def slot_copy(k, target, origin):
        return remote(
            slot_block(slots_out, target), slot_block(slots_in, origin),
            slot_send.at[k], slot_recv.at[k], {"ep": target},
        )

    def send_slots(k, carry):
        slot_copy(k, (me + k) % ep_count, me).start()
        return carry

    lax.fori_loop(1, ep_count, send_slots, 0)
    for copy in to_mate:
        copy.start()

    own_block = rows_at(me * capacity, capacity, capacity)
    slots_in[own_block, :] = slots_out[own_block, :]
    lane_ids = lax.broadcasted_iota(jnp.int32, (own, slots), 1)
    for k in range(top):
        column = jnp.broadcast_to(slot_rows[k].astype(f32), (own, own)).T[:, :1].astype(jnp.int32)
        picks[k] = (lane_ids == column).astype(f32).astype(bf16)
        weights_col[k] = jnp.broadcast_to(route[k : k + 1, lanes], (own, own)).T

    def half_copy(i, part):
        return remote(
            part.at[1 - parity], half_in.at[i], half_send.at[i], half_recv.at[i], {"tp": mate}
        )

    def last_copy(i):
        return remote(
            half_out.at[i], last_in.at[i], last_send.at[i], last_recv.at[i], {"tp": far}
        )

    def middle(i, part):
        half_copy(i, part).wait_recv()
        half_out[i] = (part[parity, 1 - level].astype(f32) + half_in[i, 1 - level].astype(f32)).astype(bf16)
        last_copy(i).start()

    for i in range(7, 14):
        loads[i].wait()
    norm_into(normed, mixer_in, 0, tokens, mixer_gain)
    pair = 2 * HEAD_DIM
    pairs = wq.shape[1] // pair
    lane = lax.broadcasted_iota(jnp.int32, (1, pair), 1)
    first_half = lane % HEAD_DIM < HEAD_DIM // 2
    lower = lane < HEAD_DIM
    twice = lax.broadcasted_iota(jnp.int32, (HEAD_DIM, pair), 0)
    twice = (lax.broadcasted_iota(jnp.int32, (HEAD_DIM, pair), 1) % HEAD_DIM == twice).astype(f32).astype(bf16)
    first_position = me % (ep_count // SEQS) * tokens
    transposed = (((1,), (1,)), ((), ()))

    def project(i, carry):
        rows = rows_at(i * WINDOW, WINDOW, WINDOW)
        ahead = rows_at((i + 1) * WINDOW, WINDOW, WINDOW)
        source = normed[rows, :]
        position = lax.broadcasted_iota(jnp.int32, (WINDOW, pair), 0) + (first_position + i * WINDOW)
        angles = position.astype(f32) * freq[...]
        cosine = jnp.cos(angles)
        sine = jnp.sin(angles)
        sine = jnp.where(first_half, -sine, sine)

        def turn(heads):
            swapped = jnp.where(
                first_half,
                pltpu.roll(heads, pair - HEAD_DIM // 2, 1),
                pltpu.roll(heads, HEAD_DIM // 2, 1),
            )
            return heads * cosine + swapped * sine

        def rounded(value):
            return value.astype(bf16).astype(f32)

        for j in range(pairs):
            cols = pl.ds(j * pair, pair)
            heads = rounded(jnp.dot(source, wq[:, cols], preferred_element_type=f32))
            queries[rows, cols] = (turn(heads).astype(bf16).astype(f32) * HEAD_DIM ** -0.5).astype(bf16)
        keys = lax.dot_general(source, wk[...], transposed, preferred_element_type=f32).astype(bf16)
        keys = jnp.dot(keys, twice, preferred_element_type=f32)
        band[0, ahead, :] = turn(keys).astype(bf16)
        values = lax.dot_general(source, wv[...], transposed, preferred_element_type=f32).astype(bf16)
        band[1, ahead, :] = jnp.dot(values, twice, preferred_element_type=f32).astype(bf16)
        return carry

    lax.fori_loop(0, tokens // WINDOW, project, 0)

    def halo_copy(target):
        return remote(
            band.at[:, pl.ds(tokens, WINDOW)], band.at[:, pl.ds(0, WINDOW)],
            halo_send, halo_recv, {"ep": target},
        )

    halo_copy((me + 1) % ep_count).start()

    norm_into(normed, rows_in, 0, tokens, gain)
    for i in (14, 15, 16):
        loads[i].wait()
    for r in range(2):
        rows = pl.ds(r * (tokens // 2), tokens // 2)
        gate = jnp.dot(normed[rows, :], sg[...], preferred_element_type=f32)
        up = jnp.dot(normed[rows, :], su[...], preferred_element_type=f32)
        shared_hidden[rows, :] = silu_times(gate, up).astype(bf16)
    for owner in range(4):
        for c in range(PIECES):
            cols = pl.ds(c * piece, piece)
            shared_part[owner % 2, owner // 2, :, cols] = jnp.dot(
                shared_hidden[pl.ds(owner * own, own), :], sd[:, cols], preferred_element_type=f32
            ).astype(bf16)
    half_copy(1, shared_part).start()

    loads[17].wait()
    halo_copy((me + 1) % ep_count).wait_recv()
    count = 2 * pairs
    row = lax.broadcasted_iota(jnp.int32, (WINDOW, 2 * WINDOW), 0)
    key = lax.broadcasted_iota(jnp.int32, (WINDOW, 2 * WINDOW), 1)
    distance = row + WINDOW - key
    in_window = (distance >= 0) & (distance < WINDOW)

    def attend(i, carry):
        rows = rows_at(i * WINDOW, WINDOW, WINDOW)
        reach = rows_at(i * WINDOW, 2 * WINDOW, WINDOW)
        allowed = in_window & (key + (first_position + (i - 1) * WINDOW) >= 0)
        keys = band[0, reach, :]
        values = band[1, reach, :]
        for j in range(pairs):
            cols = pl.ds(j * pair, pair)
            both = queries[rows, cols]
            mixed = []
            for side in range(2):
                head = 2 * j + side
                kept = jnp.where(lower if side == 0 else ~lower, both, jnp.zeros_like(both))
                scores = lax.dot_general(kept, keys, transposed, preferred_element_type=f32)
                scores = jnp.where(allowed, scores, -jnp.inf)
                sunk = sink[:, head : head + 1]
                peak = jnp.maximum(jnp.max(scores, axis=-1, keepdims=True), sunk)
                raised = jnp.exp(scores - peak)
                below = jnp.sum(raised, axis=-1, keepdims=True) + jnp.exp(sunk - peak)
                mixed.append(jnp.dot(raised.astype(bf16), values, preferred_element_type=f32) / below)
            attended[rows, cols] = jnp.where(lower, mixed[0], mixed[1]).astype(bf16)
        return carry

    lax.fori_loop(0, tokens // WINDOW, attend, 0)
    for owner in range(4):
        for c in range(PIECES):
            cols = pl.ds(c * piece, piece)
            mixer_part[owner % 2, owner // 2, :, cols] = jnp.dot(
                attended[pl.ds(owner * own, own), :], wo[:, cols], preferred_element_type=f32
            ).astype(bf16)
    half_copy(0, mixer_part).start()
    middle(0, mixer_part)
    middle(1, shared_part)

    def hidden_block(owner):
        step = 256
        columns = rows_at(owner * ff, ff, ff)

        def body(i, carry):
            rows = rows_at(i * step, step, step)
            gate = jnp.dot(slots_in[rows, :], wg[owner], preferred_element_type=f32)
            up = jnp.dot(slots_in[rows, :], wu[owner], preferred_element_type=f32)
            hidden[rows, columns] = silu_times(gate, up).astype(bf16)
            return carry

        lax.fori_loop(0, slots // step, body, 0)

    from_far[0].wait_recv()
    to_pass[0].start()

    def wait_slots(k, carry):
        slot_copy(k, me, (me + ep_count - k) % ep_count).wait_recv()
        return carry

    lax.fori_loop(1, ep_count, wait_slots, 0)
    for i in (4, 5, 6):
        loads[i].wait()
    hidden_block(t)
    for copy in from_mate:
        copy.wait_recv()
    hidden_block(mate)
    from_far[1].wait_recv()
    to_pass[1].start()
    hidden_block(far)
    for i in (0, 1):
        from_pass[i].wait_recv()
    hidden_block(far_mate)

    def back_copy(k, c, target, origin):
        cols = pl.ds(c * piece, piece)
        return remote(
            slot_block(result, target).at[:, cols], slot_block(back, origin).at[:, cols],
            back_send.at[k, c], back_recv.at[k, c], {"ep": target},
        )

    for c in range(PIECES):
        cols = pl.ds(c * piece, piece)
        from_far[2 + c].wait_recv()
        to_pass[2 + c].start()
        from_pass[2 + c].wait_recv()
        step = 256

        def down(i, carry, cols=cols):
            rows = rows_at(i * step, step, step)
            result[rows, cols] = jnp.dot(
                hidden[rows, :], wd[:, cols], preferred_element_type=f32
            ).astype(bf16)
            return carry

        lax.fori_loop(0, slots // step, down, 0)

        def send_back(k, carry, c=c):
            back_copy(k, c, (me + k) % ep_count, me).start()
            return carry

        lax.fori_loop(1, ep_count, send_back, 0)
        back[own_block, cols] = result[own_block, cols]

    def summed(i, part):
        return part[parity, level].astype(f32) + half_in[i, level].astype(f32) + last_in[i].astype(f32)

    for i in range(2):
        last_copy(i).wait_recv()
    mixer_out[...] = summed(0, mixer_part).astype(bf16)
    for c in range(PIECES):
        cols = pl.ds(c * piece, piece)

        def wait_back(k, carry, c=c):
            back_copy(k, c, me, (me + ep_count - k) % ep_count).wait_recv()
            return carry

        lax.fori_loop(1, ep_count, wait_back, 0)
        total = (
            shared_part[parity, level, :, cols].astype(f32)
            + half_in[1, level, :, cols].astype(f32)
            + last_in[1, :, cols].astype(f32)
        )
        for k in range(top):
            total = total + weights_col[k][:, :1] * jnp.dot(
                picks[k], back[:, cols], preferred_element_type=f32
            )
        expert_out[:, cols] = total.astype(bf16)

    for copy in to_far + to_mate + to_pass:
        copy.wait_send()
    for i, part in enumerate((mixer_part, shared_part)):
        half_copy(i, part).wait_send()
        last_copy(i).wait_send()

    halo_copy((me + 1) % ep_count).wait_send()

    def drain(k, carry):
        slot_copy(k, (me + k) % ep_count, me).wait_send()
        for c in range(PIECES):
            back_copy(k, c, (me + k) % ep_count, me).wait_send()
        return carry

    lax.fori_loop(1, ep_count, drain, 0)


def local(
    mixer_input,
    expert_input,
    gain_mixer,
    gain_expert,
    query_weight,
    key_weight,
    value_weight,
    sink_logits,
    output_weight,
    expert_choice,
    route_weights,
    expert_gate,
    expert_up,
    expert_down,
    shared_gate,
    shared_up,
    shared_down,
):
    tp_count = lax.axis_size("tp")
    ep_count = lax.axis_size("ep")
    tokens, width = expert_input.shape
    own = tokens // tp_count
    top = expert_choice.shape[1]
    local_experts, _, ff = expert_gate.shape
    shared_ff = shared_gate.shape[1]
    experts_all = local_experts * ep_count
    capacity = -(-(2 * own * top // experts_all) // 16) * 16
    slots = experts_all * capacity
    assert tp_count == 4 and local_experts == 1
    heads = query_weight.shape[1] // HEAD_DIM
    assert heads % 2 == 0 and key_weight.shape[1] == HEAD_DIM and own % WINDOW == 0
    hbm_spec = pl.BlockSpec(memory_space=pltpu.HBM)
    vmem_spec = pl.BlockSpec(memory_space=pltpu.VMEM)
    dma = pltpu.SemaphoreType.DMA
    vmem = pltpu.VMEM
    count = 2 + PIECES
    freq = jnp.tile(frequencies(HEAD_DIM), 4)[None, :]
    return pl.pallas_call(
        functools.partial(mixture_kernel, capacity),
        out_shape=(jax.ShapeDtypeStruct((own, width), bf16),) * 2,
        in_specs=[hbm_spec] * 18,
        out_specs=(vmem_spec,) * 2,
        scratch_shapes=[
            vmem((tokens, width), bf16),
            vmem((tokens, width), bf16),
            vmem((1, width), f32),
            vmem((top, tokens), jnp.int32),
            vmem((top, tokens), f32),
            vmem((tp_count, width, ff), bf16),
            vmem((tp_count, width, ff), bf16),
            vmem((tp_count * ff, width), bf16),
            vmem((width, shared_ff), bf16),
            vmem((width, shared_ff), bf16),
            vmem((shared_ff, width), bf16),
            vmem((tokens, width), bf16),
            vmem((1, width), f32),
            vmem(query_weight.shape, bf16),
            vmem((HEAD_DIM, width), bf16),
            vmem((HEAD_DIM, width), bf16),
            vmem(output_weight.shape, bf16),
            vmem((1, heads), f32),
            vmem((1, 2 * HEAD_DIM), f32),
            vmem((tokens, heads * HEAD_DIM), bf16),
            vmem((2, WINDOW + tokens, 2 * HEAD_DIM), bf16),
            vmem((tokens, heads * HEAD_DIM), bf16),
            vmem((own, width), bf16),
            vmem((slots, width), bf16),
            vmem((slots, width), bf16),
            vmem((slots, tp_count * ff), bf16),
            vmem((slots, width), bf16),
            vmem((slots, width), bf16),
            vmem((top, own, slots), bf16),
            vmem((top, own, own), f32),
            vmem((2, 2, own, width), bf16),
            vmem((2, 2, own, width), bf16),
            vmem((tokens, shared_ff), bf16),
            vmem((2, 2, own, width), bf16),
            vmem((2, own, width), bf16),
            vmem((2, own, width), bf16),
            dma((18,)),
            dma((count,)), dma((count,)),
            dma((count,)), dma((count,)),
            dma((count,)), dma((count,)),
            dma((ep_count,)), dma((ep_count,)),
            dma((ep_count, PIECES)), dma((ep_count, PIECES)),
            dma((2,)), dma((2,)),
            dma((2,)), dma((2,)),
            dma, dma,
        ],
        compiler_params=pltpu.CompilerParams(
            collective_id=0, has_side_effects=True, vmem_limit_bytes=56 * 1024 * 1024
        ),
    )(
        expert_input, gain_expert[None, :], expert_choice.T, route_weights.T,
        expert_gate[0], expert_up[0], expert_down[0], shared_gate, shared_up, shared_down,
        mixer_input, gain_mixer[None, :], query_weight, key_weight.T, value_weight.T, output_weight,
        sink_logits[None, :], freq,
    )


def solution(mesh):
    placed = (
        P("ep", None),
        P("ep", None),
        P(),
        P(),
        P(None, "tp"),
        P(None, "tp"),
        P(None, "tp"),
        P("tp"),
        P("tp", None),
        P("ep", None),
        P("ep", None),
        P("ep", None, "tp"),
        P("ep", None, "tp"),
        P("ep", "tp", None),
        P(None, "tp"),
        P(None, "tp"),
        P("tp", None),
    )
    return jax.shard_map(
        local,
        mesh=mesh,
        in_specs=placed,
        out_specs=(P(("ep", "tp"), None), P(("ep", "tp"), None)),
        check_vma=False,
    )
```

profile of v0, /device:TPU:9, one launch (start us, length us, event | category | flops | bytes accessed | tf_op | source)
XLA Modules:
  0.0 117.3 jit_solution(12930201134195884594)
XLA Ops:
  0.7 0.6 broadcast_in_dim_tile.3.freq_ref
  1.2 112.3 %shard_map.176 = (bf16[128,2048]{1,0:T(8,128)(2,1)}, bf16[128,2048]{1,0:T(8,128)(2,1)}) custom-call(bf16[512,2048]{1,0:T(8,128)(2,1)} %x_ref.1, f32[1,2048]{1,0:T(1,128)} %bitcast.15, s32[2,512]{1,0:T(2,128)} %bitcast.17, f32[2,512]{1,0:T(2,128)} %bitcast.18, bf16[2048,256]{1,0:T(8,128)(2,1)} %bitcast.10, bf16[2048,256]{1,0:T(8,128)(2,1)} %bitcast.11, ...), custom_call_target="tpu_custom_call" | custom-call | tf_op jit(solution)/shard_map/pallas_call | solution.py:446
  113.6 1.9 %copy.21 = bf16[128,2048]{1,0:T(8,128)(2,1)} copy(bf16[128,2048]{1,0:T(8,128)(2,1)} %get-tuple-element.4) | data formatting | bytes 1048576
  115.4 1.9 %copy.22 = bf16[128,2048]{1,0:T(8,128)(2,1)} copy(bf16[128,2048]{1,0:T(8,128)(2,1)} %get-tuple-element.5) | data formatting | bytes 1048576
  (2 shorter events, 0.0 us)
where the time goes:
time: 118 us; the launch traced here: 117 us
  Pallas kernels  112 us (95%)
  local copies, waits for them, and re-layouts  4.36 us (4%)
    pallas_call x1, Pallas kernels, local(): pl.pallas_call(functools.partial(mixture_kernel, capacity), out_shape=(ja...  112 us
    unnamed x2, local copies, waits for them, and re-layouts  3.76 us

commit v1 on v0

v1 whole, which is shorter than its diff:
```python
import functools

import jax
import jax.numpy as jnp
import numpy as np
from jax import lax
from jax.experimental import pallas as pl
from jax.experimental.pallas import tpu as pltpu
from jax.sharding import PartitionSpec as P

HEAD_DIM = 64
WINDOW = 128
SEQS = 1
PIECES = 4

norm_eps = 1e-06
rope_base = 500000.0
bf16 = jnp.bfloat16
f32 = jnp.float32
MESH = pl.DeviceIdType.MESH


def frequencies(head_size):
    half_steps = np.arange(head_size // 2, dtype=np.float64)
    return np.tile(rope_base ** (-(2.0 * half_steps) / head_size), 4).astype(np.float32)[None, :]


def rows_at(start, count, unit):
    return pl.ds(pl.multiple_of(start, unit), count)


def norm_into(target, source, to, start, count, gain):
    step = 32

    def body(i, carry):
        widened = source[rows_at(start + i * step, step, step), :].astype(f32)
        scale = lax.rsqrt(jnp.mean(widened * widened, axis=-1, keepdims=True) + norm_eps)
        target[rows_at(to + i * step, step, step), :] = (widened * scale * gain[...]).astype(bf16)
        return carry

    lax.fori_loop(0, count // step, body, 0)


def silu_times(gate, up):
    return gate / (1.0 + jnp.exp(-gate)) * up


def mixture_kernel(
    capacity,
    x_ref, gain_ref, choice_ref, route_ref,
    wg_ref, wu_ref, wd_ref, sg_ref, su_ref, sd_ref,
    mx_ref, mgain_ref, wq_ref, wk_ref, wv_ref, wo_ref, sink_ref, freq_ref,
    mixer_out, expert_out,
    rows_in, normed, gain, choice, route, wg, wu, wd, sg, su, sd,
    mixer_in, mixer_gain, wq, wk, wv, wo, sink, sunk, freq, cosines, sines, queries, band, attended,
    own_rows, slots_out, slots_in, hidden, result, back, picks, weights_col,
    mirror_choice, mirror_route, mirror_picks, mirror_weights, dense_out, dense_in, expert_sum,
    mixer_part, shared_part, shared_hidden, half_in, half_out, last_in,
    load_sem, far_send, far_recv, mate_send, mate_recv, pass_send, pass_recv,
    slot_send, slot_recv, back_send, back_recv, half_send, half_recv, last_send, last_recv,
    halo_send, halo_recv, mirror_send, mirror_recv, dense_send, dense_recv,
):
    ep_count = lax.axis_size("ep")
    me = lax.axis_index("ep")
    t = lax.axis_index("tp")
    parity = t % 2
    level = t // 2
    mate = t + 1 - 2 * parity
    far = (t + 2) % 4
    far_mate = (mate + 2) % 4
    tokens, width = rows_in.shape
    own = own_rows.shape[0]
    ff = wd_ref.shape[0]
    slots = slots_out.shape[0]
    piece = width // PIECES

    barrier = pltpu.get_barrier_semaphore()

    def greet(k, carry):
        pl.semaphore_signal(barrier, inc=1, device_id={"ep": (me + k) % ep_count}, device_id_type=MESH)
        return carry

    lax.fori_loop(1, ep_count, greet, 0)
    for other in (mate, far):
        pl.semaphore_signal(barrier, inc=1, device_id={"tp": other}, device_id_type=MESH)

    loads = [
        (gain_ref, gain), (choice_ref, choice), (route_ref, route), (x_ref, rows_in),
        (mgain_ref, mixer_gain), (freq_ref, freq), (mx_ref, mixer_in), (wk_ref, wk), (wv_ref, wv),
        (wq_ref, wq), (sink_ref, sink), (sg_ref, sg), (su_ref, su), (sd_ref, sd), (wo_ref, wo),
        (wg_ref, wg.at[t]), (wu_ref, wu.at[t]), (wd_ref, wd.at[rows_at(t * ff, ff, ff)]),
    ]
    loads = [pltpu.make_async_copy(a, b, load_sem.at[i]) for i, (a, b) in enumerate(loads)]
    for load in loads:
        load.start()

    pl.semaphore_wait(barrier, ep_count + 1)

    def block_views(owner):
        views = [wg.at[owner], wu.at[owner]]
        down = wd.at[rows_at(owner * ff, ff, ff)]
        return views + [down.at[:, pl.ds(c * piece, piece)] for c in range(PIECES)]

    sources = [wg_ref, wu_ref] + [wd_ref.at[:, pl.ds(c * piece, piece)] for c in range(PIECES)]

    def remote(src, dst, send, recv, device):
        return pltpu.make_async_remote_copy(
            src_ref=src, dst_ref=dst, send_sem=send, recv_sem=recv,
            device_id=device, device_id_type=MESH,
        )

    def views_copy(srcs, owner, send, recv, device):
        return [
            remote(a, b, send.at[i], recv.at[i], device)
            for i, (a, b) in enumerate(zip(srcs, block_views(owner)))
        ]

    to_far = views_copy(sources, t, far_send, far_recv, {"tp": far})
    to_mate = views_copy(sources, t, mate_send, mate_recv, {"tp": mate})
    from_far = views_copy(sources, far, far_send, far_recv, {"tp": far})
    from_mate = views_copy(sources, mate, mate_send, mate_recv, {"tp": mate})
    to_pass = views_copy(block_views(far), far, pass_send, pass_recv, {"tp": mate})
    from_pass = views_copy(block_views(far), far_mate, pass_send, pass_recv, {"tp": mate})
    for copy in to_far:
        copy.start()

    for i in (0, 1, 2, 3):
        loads[i].wait()
    norm_into(own_rows, rows_in, 0, t * own, own, gain)
    lanes = rows_at(t * own, own, own)
    top = choice.shape[0]
    row_ids = lax.broadcasted_iota(jnp.int32, (slots // capacity, own), 0)
    earlier = lax.broadcasted_iota(jnp.int32, (own, own), 0)
    later = lax.broadcasted_iota(jnp.int32, (own, own), 1)
    before = (earlier < later).astype(f32)

    def slots_of(choices):
        chosen = choices[:, lanes]
        named = [row_ids == chosen[k : k + 1, :] for k in range(top)]
        named_any = functools.reduce(jnp.logical_or, named).astype(f32)
        ranks = jnp.dot(named_any, before, preferred_element_type=f32)
        return [
            chosen[k : k + 1, :] * capacity
            + jnp.sum(jnp.where(named[k], ranks, 0.0), axis=0, keepdims=True).astype(jnp.int32)
            for k in range(top)
        ]

    def column_of(row):
        return jnp.broadcast_to(row.astype(f32), (own, own)).T

    slot_rows = slots_of(choice)
    slot_ids = lax.broadcasted_iota(jnp.int32, (slots, own), 0)
    spread = functools.reduce(jnp.logical_or, [slot_ids == row for row in slot_rows])
    spread = spread.astype(f32).astype(bf16)
    for c in range(PIECES):
        cols = pl.ds(c * piece, piece)
        slots_out[:, cols] = jnp.dot(spread, own_rows[:, cols], preferred_element_type=f32).astype(bf16)

    def slot_block(ref, owner):
        return ref.at[rows_at(owner * capacity, capacity, capacity)]

    def slot_copy(k, target, origin):
        return remote(
            slot_block(slots_out, target), slot_block(slots_in, origin),
            slot_send.at[k], slot_recv.at[k], {"ep": target},
        )

    def send_slots(k, carry):
        slot_copy(k, (me + k) % ep_count, me).start()
        return carry

    ahead_of_halo = ep_count // 2
    lax.fori_loop(ep_count // 4, ahead_of_halo, send_slots, 0)

    for i in range(4, 9):
        loads[i].wait()
    pair = 2 * HEAD_DIM
    lane = lax.broadcasted_iota(jnp.int32, (1, pair), 1)
    first_half = lane % HEAD_DIM < HEAD_DIM // 2
    lower = lane < HEAD_DIM
    twice = lax.broadcasted_iota(jnp.int32, (HEAD_DIM, pair), 0)
    twice = (lax.broadcasted_iota(jnp.int32, (HEAD_DIM, pair), 1) % HEAD_DIM == twice).astype(f32).astype(bf16)
    first_position = me % (ep_count // SEQS) * tokens
    transposed = (((1,), (1,)), ((), ()))

    def turn(heads, rows):
        swapped = jnp.where(
            first_half,
            pltpu.roll(heads, pair - HEAD_DIM // 2, 1),
            pltpu.roll(heads, HEAD_DIM // 2, 1),
        )
        return heads * cosines[rows, :] + swapped * sines[rows, :]

    def project_keys(i, carry):
        rows = rows_at(i * WINDOW, WINDOW, WINDOW)
        after = rows_at((i + 1) * WINDOW, WINDOW, WINDOW)
        norm_into(normed, mixer_in, i * WINDOW, i * WINDOW, WINDOW, mixer_gain)
        position = lax.broadcasted_iota(jnp.int32, (WINDOW, pair), 0) + (first_position + i * WINDOW)
        angles = position.astype(f32) * freq[...]
        sine = jnp.sin(angles)
        cosines[rows, :] = jnp.cos(angles)
        sines[rows, :] = jnp.where(first_half, -sine, sine)
        source = normed[rows, :]
        keys = lax.dot_general(source, wk[...], transposed, preferred_element_type=f32).astype(bf16)
        keys = jnp.dot(keys, twice, preferred_element_type=f32)
        band[0, after, :] = turn(keys, rows).astype(bf16)
        values = lax.dot_general(source, wv[...], transposed, preferred_element_type=f32).astype(bf16)
        band[1, after, :] = jnp.dot(values, twice, preferred_element_type=f32).astype(bf16)
        return carry

    def halo_copy(target):
        return remote(
            band.at[:, pl.ds(tokens, WINDOW)], band.at[:, pl.ds(0, WINDOW)],
            halo_send, halo_recv, {"ep": target},
        )

    last_block = tokens // WINDOW - 1
    project_keys(last_block, 0)
    halo_copy((me + 1) % ep_count).start()
    lax.fori_loop(ahead_of_halo, ep_count, send_slots, 0)
    lax.fori_loop(1, ep_count // 4, send_slots, 0)
    for copy in to_mate:
        copy.start()

    quarter_size = ep_count // 4
    quarter = me // quarter_size
    seat = me % quarter_size
    high = quarter // 2
    middle_one = (quarter + high) % 2
    mirror = (3 - quarter) * quarter_size + seat
    side_rows = 2 * quarter_size * capacity
    mirrored = [
        remote(a, b, mirror_send.at[i], mirror_recv.at[i], {"ep": mirror})
        for i, (a, b) in enumerate(((choice, mirror_choice), (route, mirror_route)))
    ]
    for copy in mirrored:
        copy.start()
    own_block = rows_at(me * capacity, capacity, capacity)
    slots_in[own_block, :] = slots_out[own_block, :]
    lane_ids = lax.broadcasted_iota(jnp.int32, (own, slots), 1)
    for k in range(top):
        picks[k] = (lane_ids == column_of(slot_rows[k])[:, :1].astype(jnp.int32)).astype(f32).astype(bf16)
        weights_col[k] = column_of(route[k : k + 1, lanes])

    @pl.when(middle_one == 1)
    def _():
        back[rows_at((1 - high) * side_rows, side_rows, capacity), :] = jnp.zeros((side_rows, width), bf16)

    @pl.when(middle_one == 0)
    def _():
        dense_in[...] = jnp.zeros((own, width), bf16)

    def half_copy(i, part):
        return remote(
            part.at[1 - parity], half_in.at[i], half_send.at[i], half_recv.at[i], {"tp": mate}
        )

    def last_copy(i):
        return remote(
            half_out.at[i], last_in.at[i], last_send.at[i], last_recv.at[i], {"tp": far}
        )

    def middle(i, part):
        half_copy(i, part).wait_recv()
        half_out[i] = (part[parity, 1 - level].astype(f32) + half_in[i, 1 - level].astype(f32)).astype(bf16)
        last_copy(i).start()

    lax.fori_loop(0, last_block, project_keys, 0)
    loads[9].wait()
    pairs = wq.shape[1] // pair

    def project(i, carry):
        rows = rows_at(i * WINDOW, WINDOW, WINDOW)
        for j in range(pairs):
            cols = pl.ds(j * pair, pair)
            heads = jnp.dot(normed[rows, :], wq[:, cols], preferred_element_type=f32)
            turned_heads = turn(heads.astype(bf16).astype(f32), rows).astype(bf16)
            queries[rows, cols] = (turned_heads.astype(f32) * HEAD_DIM ** -0.5).astype(bf16)
        return carry

    lax.fori_loop(0, tokens // WINDOW, project, 0)

    norm_into(normed, rows_in, 0, 0, tokens, gain)
    for i in (11, 12, 13):
        loads[i].wait()
    for r in range(2):
        rows = pl.ds(r * (tokens // 2), tokens // 2)
        gate = jnp.dot(normed[rows, :], sg[...], preferred_element_type=f32)
        up = jnp.dot(normed[rows, :], su[...], preferred_element_type=f32)
        shared_hidden[rows, :] = silu_times(gate, up).astype(bf16)
    for owner in range(4):
        for c in range(PIECES):
            cols = pl.ds(c * piece, piece)
            shared_part[owner % 2, owner // 2, :, cols] = jnp.dot(
                shared_hidden[pl.ds(owner * own, own), :], sd[:, cols], preferred_element_type=f32
            ).astype(bf16)
    half_copy(1, shared_part).start()

    for i in (10, 14):
        loads[i].wait()
    halo_copy((me + 1) % ep_count).wait_recv()
    count = 2 * pairs
    row = lax.broadcasted_iota(jnp.int32, (WINDOW, 2 * WINDOW), 0)
    key = lax.broadcasted_iota(jnp.int32, (WINDOW, 2 * WINDOW), 1)
    distance = row + WINDOW - key
    in_window = (distance >= 0) & (distance < WINDOW)

    for head in range(count):
        sunk[pl.ds(head * WINDOW, WINDOW), :] = jnp.broadcast_to(sink[:, head : head + 1], (WINDOW, pair))

    def attend(i, carry):
        rows = rows_at(i * WINDOW, WINDOW, WINDOW)
        reach = rows_at(i * WINDOW, 2 * WINDOW, WINDOW)
        allowed = in_window & (key + (first_position + (i - 1) * WINDOW) >= 0)
        both = [queries[rows, pl.ds(j * pair, pair)] for j in range(pairs)]
        none = jnp.zeros((WINDOW, pair), bf16)
        kept = jnp.concatenate(
            [jnp.where(side, heads, none) for heads in both for side in (lower, ~lower)], axis=0
        )
        scores = lax.dot_general(kept, band[0, reach, :], transposed, preferred_element_type=f32)
        scores = jnp.where(allowed[None], scores.reshape(count, WINDOW, 2 * WINDOW), -jnp.inf)
        scores = scores.reshape(count * WINDOW, 2 * WINDOW)
        sinks = sunk[:, :1]
        peak = jnp.maximum(jnp.max(scores, axis=-1, keepdims=True), sinks)
        raised = jnp.exp(scores - peak).astype(bf16)
        values = jnp.concatenate([band[1, reach, :], jnp.ones((2 * WINDOW, pair), bf16)], axis=1)
        mixed = jnp.dot(raised, values, preferred_element_type=f32)
        mixed = (mixed[:, :pair] / (mixed[:, pair:] + jnp.exp(sinks - peak))).reshape(count, WINDOW, pair)
        for j in range(pairs):
            attended[rows, pl.ds(j * pair, pair)] = jnp.where(
                lower, mixed[2 * j], mixed[2 * j + 1]
            ).astype(bf16)
        return carry

    lax.fori_loop(0, tokens // WINDOW, attend, 0)
    for owner in range(4):
        for c in range(PIECES):
            cols = pl.ds(c * piece, piece)
            mixer_part[owner % 2, owner // 2, :, cols] = jnp.dot(
                attended[pl.ds(owner * own, own), :], wo[:, cols], preferred_element_type=f32
            ).astype(bf16)
    half_copy(0, mixer_part).start()
    middle(0, mixer_part)
    middle(1, shared_part)

    def hidden_block(owner, side):
        rows = rows_at(side * side_rows, side_rows, capacity)
        gate = jnp.dot(slots_in[rows, :], wg[owner], preferred_element_type=f32)
        up = jnp.dot(slots_in[rows, :], wu[owner], preferred_element_type=f32)
        hidden[rows, rows_at(owner * ff, ff, ff)] = silu_times(gate, up).astype(bf16)

    from_far[0].wait_recv()
    to_pass[0].start()

    def wait_slots(side):
        def wait_one(k, carry):
            source = (me + ep_count - k) % ep_count

            @pl.when(source // (2 * quarter_size) == side)
            def _():
                slot_copy(k, me, source).wait_recv()

            return carry

        lax.fori_loop(1, ep_count, wait_one, 0)

    wait_slots(high)
    for i in (15, 16, 17):
        loads[i].wait()
    hidden_block(t, high)
    for copy in from_mate:
        copy.wait_recv()
    hidden_block(mate, high)
    from_far[1].wait_recv()
    to_pass[1].start()
    hidden_block(far, high)
    wait_slots(1 - high)
    hidden_block(t, 1 - high)
    hidden_block(mate, 1 - high)
    hidden_block(far, 1 - high)
    for i in (0, 1):
        from_pass[i].wait_recv()
    hidden_block(far_mate, high)
    hidden_block(far_mate, 1 - high)

    def is_low_middle(q):
        return (q % 2) * (1 - q // 2)

    def is_high_middle(q):
        return (q // 2) * (1 - q % 2)

    def turned(source, target):
        return is_low_middle(target) * (source // 2) + is_high_middle(target) * (1 - source // 2)

    def landing(source, source_seat, target):
        stop = turned(source, target)
        straight = source * quarter_size + source_seat
        return (1 - stop) * straight + stop * (ep_count + (source % 2) * quarter_size + source_seat)

    def back_copy(k, c, owner, target, block):
        cols = pl.ds(c * piece, piece)
        return remote(
            slot_block(result, owner).at[:, cols], slot_block(back, block).at[:, cols],
            back_send.at[k, c], back_recv.at[block, c], {"ep": target},
        )

    def each_back(c, remote_do, local_do):
        for n, q in enumerate((1, 0, 2, 3)):
            target = high * q + (1 - high) * (3 - q)
            stop = turned(quarter, target)
            via = target + stop * (2 * high - 1)

            def step(j, carry, n=n, target=target, via=via):
                to_seat = (seat + j) % quarter_size
                owner = target * quarter_size + to_seat
                device = via * quarter_size + to_seat
                block = landing(quarter, seat, target)

                @pl.when(device != me)
                def _():
                    remote_do(back_copy(n * quarter_size + j, c, owner, device, block))

                if local_do is not None:
                    @pl.when(device == me)
                    def _():
                        local_do(owner, block)

                return carry

            lax.fori_loop(0, quarter_size, step, 0)

    def wait_block(c, block):
        back_copy(0, c, me, me, block).wait_recv()

    def dense_copy(c):
        cols = pl.ds(c * piece, piece)
        return remote(
            dense_out.at[:, cols], dense_in.at[:, cols], dense_send.at[c], dense_recv.at[c], {"ep": mirror}
        )

    def relay(c):
        cols = pl.ds(c * piece, piece)

        @pl.when(middle_one == 1)
        def _():
            def wait_relayed(n, carry):
                @pl.when(n != (quarter % 2) * quarter_size + seat)
                def _():
                    wait_block(c, ep_count + n)

                return carry

            lax.fori_loop(0, 2 * quarter_size, wait_relayed, 0)
            total = 0.0
            for k in range(top):
                total = total + mirror_weights[k][:, :1] * jnp.dot(
                    mirror_picks[k], back[pl.ds(slots, side_rows), cols], preferred_element_type=f32
                )
            dense_out[:, cols] = total.astype(bf16)
            dense_copy(c).start()

    for copy in mirrored:
        copy.wait_recv()
    near_ids = lax.broadcasted_iota(jnp.int32, (own, side_rows), 1) + high * side_rows
    for k, row in enumerate(slots_of(mirror_choice)):
        mirror_picks[k] = (near_ids == column_of(row)[:, :1].astype(jnp.int32)).astype(f32).astype(bf16)
        mirror_weights[k] = column_of(mirror_route[k : k + 1, lanes])

    for c in range(PIECES):
        cols = pl.ds(c * piece, piece)
        from_far[2 + c].wait_recv()
        to_pass[2 + c].start()
        from_pass[2 + c].wait_recv()
        step = 256

        def down(i, carry, cols=cols):
            rows = rows_at(i * step, step, step)
            result[rows, cols] = jnp.dot(
                hidden[rows, :], wd[:, cols], preferred_element_type=f32
            ).astype(bf16)
            return carry

        lax.fori_loop(0, slots // step, down, 0)

        def keep(owner, block, cols=cols):
            back[rows_at(block * capacity, capacity, capacity), cols] = result[
                rows_at(owner * capacity, capacity, capacity), cols
            ]

        each_back(c, lambda copy: copy.start(), keep)
        if c > 0:
            relay(c - 1)
    relay(PIECES - 1)

    def summed(i, part):
        return part[parity, level].astype(f32) + half_in[i, level].astype(f32) + last_in[i].astype(f32)

    for c in range(PIECES):
        cols = pl.ds(c * piece, piece)

        def wait_back(k, carry, c=c):
            source = (me + ep_count - k) % ep_count

            @pl.when(turned(source // quarter_size, quarter) == 0)
            def _():
                wait_block(c, source)

            return carry

        lax.fori_loop(1, ep_count, wait_back, 0)

        @pl.when(middle_one == 1)
        def _(c=c):
            dense_copy(c).wait_recv()

        total = (
            shared_part[parity, level, :, cols].astype(f32)
            + half_in[1, level, :, cols].astype(f32)
            + dense_in[:, cols].astype(f32)
        )
        for k in range(top):
            total = total + weights_col[k][:, :1] * jnp.dot(
                picks[k], back[pl.ds(0, slots), cols], preferred_element_type=f32
            )
        expert_sum[:, cols] = total
    last_copy(0).wait_recv()
    mixer_out[...] = summed(0, mixer_part)
    last_copy(1).wait_recv()
    expert_out[...] = expert_sum[...] + last_in[1].astype(f32)

    for copy in to_far + to_mate + to_pass:
        copy.wait_send()
    for i, part in enumerate((mixer_part, shared_part)):
        half_copy(i, part).wait_send()
        last_copy(i).wait_send()

    halo_copy((me + 1) % ep_count).wait_send()

    def drain(k, carry):
        slot_copy(k, (me + k) % ep_count, me).wait_send()
        return carry

    lax.fori_loop(1, ep_count, drain, 0)
    for copy in mirrored:
        copy.wait_send()
    for c in range(PIECES):
        each_back(c, lambda copy: copy.wait_send(), None)

        @pl.when(middle_one == 1)
        def _(c=c):
            dense_copy(c).wait_send()


def local(
    mixer_input,
    expert_input,
    gain_mixer,
    gain_expert,
    query_weight,
    key_weight,
    value_weight,
    sink_logits,
    output_weight,
    expert_choice,
    route_weights,
    expert_gate,
    expert_up,
    expert_down,
    shared_gate,
    shared_up,
    shared_down,
):
    tp_count = lax.axis_size("tp")
    ep_count = lax.axis_size("ep")
    tokens, width = expert_input.shape
    own = tokens // tp_count
    top = expert_choice.shape[1]
    local_experts, _, ff = expert_gate.shape
    shared_ff = shared_gate.shape[1]
    experts_all = local_experts * ep_count
    capacity = -(-(2 * own * top // experts_all) // 16) * 16
    slots = experts_all * capacity
    side_rows = slots // 2
    assert tp_count == 4 and local_experts == 1 and ep_count % 4 == 0
    heads = query_weight.shape[1] // HEAD_DIM
    assert heads % 2 == 0 and key_weight.shape[1] == HEAD_DIM and own % WINDOW == 0
    hbm_spec = pl.BlockSpec(memory_space=pltpu.HBM)
    vmem_spec = pl.BlockSpec(memory_space=pltpu.VMEM)
    dma = pltpu.SemaphoreType.DMA
    vmem = pltpu.VMEM
    count = 2 + PIECES
    sums = pl.pallas_call(
        functools.partial(mixture_kernel, capacity),
        out_shape=(jax.ShapeDtypeStruct((own, width), f32),) * 2,
        in_specs=[hbm_spec] * 18,
        out_specs=(vmem_spec,) * 2,
        scratch_shapes=[
            vmem((tokens, width), bf16),
            vmem((tokens, width), bf16),
            vmem((1, width), f32),
            vmem((top, tokens), jnp.int32),
            vmem((top, tokens), f32),
            vmem((tp_count, width, ff), bf16),
            vmem((tp_count, width, ff), bf16),
            vmem((tp_count * ff, width), bf16),
            vmem((width, shared_ff), bf16),
            vmem((width, shared_ff), bf16),
            vmem((shared_ff, width), bf16),
            vmem((tokens, width), bf16),
            vmem((1, width), f32),
            vmem(query_weight.shape, bf16),
            vmem((HEAD_DIM, width), bf16),
            vmem((HEAD_DIM, width), bf16),
            vmem(output_weight.shape, bf16),
            vmem((1, heads), f32),
            vmem((heads * WINDOW, 2 * HEAD_DIM), f32),
            vmem((1, 2 * HEAD_DIM), f32),
            vmem((tokens, 2 * HEAD_DIM), f32),
            vmem((tokens, 2 * HEAD_DIM), f32),
            vmem((tokens, heads * HEAD_DIM), bf16),
            vmem((2, WINDOW + tokens, 2 * HEAD_DIM), bf16),
            vmem((tokens, heads * HEAD_DIM), bf16),
            vmem((own, width), bf16),
            vmem((slots, width), bf16),
            vmem((slots, width), bf16),
            vmem((slots, tp_count * ff), bf16),
            vmem((slots, width), bf16),
            vmem((slots + side_rows, width), bf16),
            vmem((top, own, slots), bf16),
            vmem((top, own, own), f32),
            vmem((top, tokens), jnp.int32),
            vmem((top, tokens), f32),
            vmem((top, own, side_rows), bf16),
            vmem((top, own, own), f32),
            vmem((own, width), bf16),
            vmem((own, width), bf16),
            vmem((own, width), f32),
            vmem((2, 2, own, width), bf16),
            vmem((2, 2, own, width), bf16),
            vmem((tokens, shared_ff), bf16),
            vmem((2, 2, own, width), bf16),
            vmem((2, own, width), bf16),
            vmem((2, own, width), bf16),
            dma((18,)),
            dma((count,)), dma((count,)),
            dma((count,)), dma((count,)),
            dma((count,)), dma((count,)),
            dma((ep_count,)), dma((ep_count,)),
            dma((ep_count, PIECES)), dma((ep_count + ep_count // 2, PIECES)),
            dma((2,)), dma((2,)),
            dma((2,)), dma((2,)),
            dma, dma,
            dma((2,)), dma((2,)),
            dma((PIECES,)), dma((PIECES,)),
        ],
        compiler_params=pltpu.CompilerParams(
            collective_id=0, has_side_effects=True, vmem_limit_bytes=62 * 1024 * 1024
        ),
    )(
        expert_input, gain_expert[None, :], expert_choice.T, route_weights.T,
        expert_gate[0], expert_up[0], expert_down[0], shared_gate, shared_up, shared_down,
        mixer_input, gain_mixer[None, :], query_weight, key_weight.T, value_weight.T, output_weight,
        sink_logits[None, :], frequencies(HEAD_DIM),
    )
    return tuple(value.astype(bf16) for value in sums)


def solution(mesh):
    placed = (
        P("ep", None),
        P("ep", None),
        P(),
        P(),
        P(None, "tp"),
        P(None, "tp"),
        P(None, "tp"),
        P("tp"),
        P("tp", None),
        P("ep", None),
        P("ep", None),
        P("ep", None, "tp"),
        P("ep", None, "tp"),
        P("ep", "tp", None),
        P(None, "tp"),
        P(None, "tp"),
        P("tp", None),
    )
    return jax.shard_map(
        local,
        mesh=mesh,
        in_specs=placed,
        out_specs=(P(("ep", "tp"), None), P(("ep", "tp"), None)),
        check_vma=False,
    )
```

time: 118 us -> 105 us (0.89)
  Pallas kernels: 112 us -> 99.7 us
  local copies, waits for them, and re-layouts: 4.36 us -> 0.01 us
  other arithmetic: 0.01 us -> 3.03 us
    pallas_call x1, Pallas kernels: 112 us -> 99.7 us  [local(): pl.pallas_call(functools.partial(mixture_kernel, capacity), out_shape=(ja...]
    unnamed x2, local copies, waits for them, and re-layouts: 3.76 us -> 0.01 us
    convert_element_type x0 -> x2, other arithmetic: none -> 3.03 us  [local(): return tuple((value.astype(bf16) for value in sums))]
where the time goes in v1:
time: 105 us; the launch traced here: 103 us
  Pallas kernels  99.7 us (95%)
  other arithmetic  3.03 us (3%)
    pallas_call x1, Pallas kernels, local(): pl.pallas_call(functools.partial(mixture_kernel, capacity), out_shape=(ja...  99.7 us
    convert_element_type x2, other arithmetic, local(): return tuple((value.astype(bf16) for value in sums))  3.03 us

profile of v1, /device:TPU:9, one launch (start us, length us, event | category | flops | bytes accessed | tf_op | source)
XLA Modules:
  0.0 103.3 jit_solution(1899723455092395469)
XLA Ops:
  0.6 99.7 %shard_map.185 = (f32[128,2048]{1,0:T(8,128)}, f32[128,2048]{1,0:T(8,128)}) custom-call(bf16[512,2048]{1,0:T(8,128)(2,1)} %x_ref.1, f32[1,2048]{1,0:T(1,128)} %bitcast.15, s32[2,512]{1,0:T(2,128)} %bitcast.17, f32[2,512]{1,0:T(2,128)} %bitcast.18, bf16[2048,256]{1,0:T(8,128)(2,1)} %bitcast.10, bf16[2048,256]{1,0:T(8,128)(2,1)} %bitcast.11, ...), custom_call_target="tpu_custom_call" | custom-call | tf_op jit(solution)/shard_map/pallas_call | solution.py:592
  100.3 0.0 copy-start
  100.3 2.2 %convert_element_type.6 = bf16[128,2048]{1,0:T(8,128)(2,1)} convert(f32[128,2048]{1,0:T(8,128)} %get-tuple-element.4) | non-fusion elementwise | flops 262144 | bytes 1572864 | tf_op jit(solution)/shard_map/convert_element_type | solution.py:665
  102.5 0.0 copy-done
  102.5 0.9 convert_element_type.7
Async XLA Ops:
  100.3 2.2 %copy-start = (f32[128,2048]{1,0:T(8,128)S(1)}, f32[128,2048]{1,0:T(8,128)}, u32[]{:S(2)}) copy-start(f32[128,2048]{1,0:T(8,128)} %get-tuple-element.5) | copy-start | bytes 3145732

commit v2 on v1

--- a/solution.py
+++ b/solution.py
@@ -11,7 +11,10 @@
 HEAD_DIM = 64
 WINDOW = 128
 SEQS = 1
-PIECES = 4
+PIECES = 8
+BLOCKS = 4
+LAG = 2
+EARLY = 6
 
 norm_eps = 1e-06
 rope_base = 500000.0
@@ -51,14 +54,15 @@
     wg_ref, wu_ref, wd_ref, sg_ref, su_ref, sd_ref,
     mx_ref, mgain_ref, wq_ref, wk_ref, wv_ref, wo_ref, sink_ref, freq_ref,
     mixer_out, expert_out,
-    rows_in, normed, gain, choice, route, wg, wu, wd, sg, su, sd,
+    rows_in, normed, gain, choice, route, wgu, wd, sg, su, sd,
     mixer_in, mixer_gain, wq, wk, wv, wo, sink, sunk, freq, cosines, sines, queries, band, attended,
     own_rows, slots_out, slots_in, hidden, result, back, picks, weights_col,
     mirror_choice, mirror_route, mirror_picks, mirror_weights, dense_out, dense_in, expert_sum,
-    mixer_part, shared_part, shared_hidden, half_in, half_out, last_in,
+    mixer_part, shared_hidden, shared_all, half_in, half_out, last_in, mirror_rows, mirror_slots,
     load_sem, far_send, far_recv, mate_send, mate_recv, pass_send, pass_recv,
     slot_send, slot_recv, back_send, back_recv, half_send, half_recv, last_send, last_recv,
     halo_send, halo_recv, mirror_send, mirror_recv, dense_send, dense_recv,
+    dealt_send, row_send, row_recv, hid_send, hid_recv, sd_send, sd_recv,
 ):
     ep_count = lax.axis_size("ep")
     me = lax.axis_index("ep")
@@ -70,7 +74,16 @@
     far_mate = (mate + 2) % 4
     tokens, width = rows_in.shape
     own = own_rows.shape[0]
+    quarter_size = ep_count // 4
+    quarter = me // quarter_size
+    seat = me % quarter_size
+    high = quarter // 2
+    middle_one = (quarter + high) % 2
+    mirror = (3 - quarter) * quarter_size + seat
+    side_rows = 2 * quarter_size * capacity
     ff = wd_ref.shape[0]
+    shared_ff = sd_ref.shape[0]
+    block = width // BLOCKS
     slots = slots_out.shape[0]
     piece = width // PIECES
 
@@ -81,27 +94,37 @@
         return carry
 
     lax.fori_loop(1, ep_count, greet, 0)
-    for other in (mate, far):
+    for other in (mate, far, far_mate):
         pl.semaphore_signal(barrier, inc=1, device_id={"tp": other}, device_id_type=MESH)
+
+    part = ff // 2
+    halves = [pl.ds(h * part, part) for h in range(2)]
+    gate_up_sources = [ref.at[:, half] for half in halves for ref in (wg_ref, wu_ref)]
+    sources = gate_up_sources + [wd_ref.at[:, pl.ds(c * piece, piece)] for c in range(PIECES)]
+
+    def gate_up_views(owner):
+        return [wgu.at[owner, i] for i in range(4)]
+
+    wide = width // 2
+
+    def sd_view(owner, half):
+        return sd.at[half, rows_at(owner * shared_ff, shared_ff, shared_ff)]
+
+    def block_views(owner):
+        return gate_up_views(owner) + [wd.at[c, rows_at(owner * ff, ff, ff)] for c in range(PIECES)]
 
     loads = [
         (gain_ref, gain), (choice_ref, choice), (route_ref, route), (x_ref, rows_in),
         (mgain_ref, mixer_gain), (freq_ref, freq), (mx_ref, mixer_in), (wk_ref, wk), (wv_ref, wv),
-        (wq_ref, wq), (sink_ref, sink), (sg_ref, sg), (su_ref, su), (sd_ref, sd), (wo_ref, wo),
-        (wg_ref, wg.at[t]), (wu_ref, wu.at[t]), (wd_ref, wd.at[rows_at(t * ff, ff, ff)]),
+        (wq_ref, wq), (sink_ref, sink), (sg_ref, sg), (su_ref, su), (wo_ref, wo),
     ]
+    loads += [(sd_ref.at[:, pl.ds(h * wide, wide)], sd_view(t, h)) for h in range(2)]
+    loads += list(zip(sources, block_views(t)))
     loads = [pltpu.make_async_copy(a, b, load_sem.at[i]) for i, (a, b) in enumerate(loads)]
     for load in loads:
         load.start()
 
-    pl.semaphore_wait(barrier, ep_count + 1)
-
-    def block_views(owner):
-        views = [wg.at[owner], wu.at[owner]]
-        down = wd.at[rows_at(owner * ff, ff, ff)]
-        return views + [down.at[:, pl.ds(c * piece, piece)] for c in range(PIECES)]
-
-    sources = [wg_ref, wu_ref] + [wd_ref.at[:, pl.ds(c * piece, piece)] for c in range(PIECES)]
+    pl.semaphore_wait(barrier, ep_count + 2)
 
     def remote(src, dst, send, recv, device):
         return pltpu.make_async_remote_copy(
@@ -121,11 +144,47 @@
     from_mate = views_copy(sources, mate, mate_send, mate_recv, {"tp": mate})
     to_pass = views_copy(block_views(far), far, pass_send, pass_recv, {"tp": mate})
     from_pass = views_copy(block_views(far), far_mate, pass_send, pass_recv, {"tp": mate})
-    for copy in to_far:
+    side_bit = me % 2
+    beside = me + 1 - 2 * side_bit
+    sd_to_far = remote(
+        sd_ref.at[:, rows_at(side_bit * wide, wide, wide)], sd_view(t, side_bit),
+        sd_send.at[0], sd_recv.at[0], {"tp": far},
+    )
+    sd_from_far = remote(sd_view(far, side_bit), sd_view(far, side_bit), sd_send.at[0], sd_recv.at[0], {"tp": far})
+    sd_to_beside = remote(sd_view(far, side_bit), sd_view(far, side_bit), sd_send.at[1], sd_recv.at[1], {"ep": beside})
+    sd_from_beside = remote(sd_view(far, 1 - side_bit), sd_view(far, 1 - side_bit), sd_send.at[1], sd_recv.at[1], {"ep": beside})
+    sd_to_mate, sd_from_mate = (
+        [
+            remote(sd_ref.at[:, pl.ds(h * wide, wide)], sd_view(owner, h), sd_send.at[4 + h], sd_recv.at[4 + h], {"tp": mate})
+            for h in range(2)
+        ]
+        for owner in (t, mate)
+    )
+    sd_passed = [
+        (
+            remote(sd_view(far, half), sd_view(far, half), sd_send.at[2 + i], sd_recv.at[2 + i], {"tp": mate}),
+            remote(sd_view(far_mate, half), sd_view(far_mate, half), sd_send.at[2 + i], sd_recv.at[2 + i], {"tp": mate}),
+        )
+        for i, half in enumerate((side_bit, 1 - side_bit))
+    ]
+    for copy in to_far[: 4 + EARLY]:
+        copy.start()
+    sd_to_far.start()
+    for copy in to_far[4 + EARLY :]:
         copy.start()
 
     for i in (0, 1, 2, 3):
         loads[i].wait()
+    mirrored = [
+        remote(a, b, mirror_send.at[i], mirror_recv.at[i], {"ep": mirror})
+        for i, (a, b) in enumerate(((choice, mirror_choice), (route, mirror_route)))
+    ]
+
+    @pl.when(middle_one == 1)
+    def _():
+        for copy in mirrored:
+            copy.start()
+
     norm_into(own_rows, rows_in, 0, t * own, own, gain)
     lanes = rows_at(t * own, own, own)
     top = choice.shape[0]
@@ -152,8 +211,8 @@
     slot_ids = lax.broadcasted_iota(jnp.int32, (slots, own), 0)
     spread = functools.reduce(jnp.logical_or, [slot_ids == row for row in slot_rows])
     spread = spread.astype(f32).astype(bf16)
-    for c in range(PIECES):
-        cols = pl.ds(c * piece, piece)
+    for c in range(BLOCKS):
+        cols = pl.ds(c * block, block)
         slots_out[:, cols] = jnp.dot(spread, own_rows[:, cols], preferred_element_type=f32).astype(bf16)
 
     def slot_block(ref, owner):
@@ -165,12 +224,24 @@
             slot_send.at[k], slot_recv.at[k], {"ep": target},
         )
 
-    def send_slots(k, carry):
-        slot_copy(k, (me + k) % ep_count, me).start()
+    rows_copy = remote(own_rows, mirror_rows, row_send, row_recv, {"ep": mirror})
+
+    def send_slots(side, k):
+        target = (me + k) % ep_count
+
+        @pl.when(target // (2 * quarter_size) == side)
+        def _():
+            slot_copy(k, target, me).start()
+
+    def send_near(k, carry):
+        send_slots(high, k)
         return carry
 
-    ahead_of_halo = ep_count // 2
-    lax.fori_loop(ep_count // 4, ahead_of_halo, send_slots, 0)
+    def send_far(k, carry):
+        send_slots(1 - high, k)
+        return carry
+
+    lax.fori_loop(1, ep_count, send_near, 0)
 
     for i in range(4, 9):
         loads[i].wait()
@@ -217,24 +288,14 @@
     last_block = tokens // WINDOW - 1
     project_keys(last_block, 0)
     halo_copy((me + 1) % ep_count).start()
-    lax.fori_loop(ahead_of_halo, ep_count, send_slots, 0)
-    lax.fori_loop(1, ep_count // 4, send_slots, 0)
-    for copy in to_mate:
+
+    @pl.when(middle_one == 1)
+    def _():
+        rows_copy.start()
+
+    for copy in to_mate + sd_to_mate:
         copy.start()
 
-    quarter_size = ep_count // 4
-    quarter = me // quarter_size
-    seat = me % quarter_size
-    high = quarter // 2
-    middle_one = (quarter + high) % 2
-    mirror = (3 - quarter) * quarter_size + seat
-    side_rows = 2 * quarter_size * capacity
-    mirrored = [
-        remote(a, b, mirror_send.at[i], mirror_recv.at[i], {"ep": mirror})
-        for i, (a, b) in enumerate(((choice, mirror_choice), (route, mirror_route)))
-    ]
-    for copy in mirrored:
-        copy.start()
     own_block = rows_at(me * capacity, capacity, capacity)
     slots_in[own_block, :] = slots_out[own_block, :]
     lane_ids = lax.broadcasted_iota(jnp.int32, (own, slots), 1)
@@ -244,26 +305,15 @@
 
     @pl.when(middle_one == 1)
     def _():
-        back[rows_at((1 - high) * side_rows, side_rows, capacity), :] = jnp.zeros((side_rows, width), bf16)
+        for c in range(PIECES):
+            back[c, rows_at((1 - high) * side_rows, side_rows, capacity), :] = jnp.zeros((side_rows, piece), bf16)
 
     @pl.when(middle_one == 0)
     def _():
-        dense_in[...] = jnp.zeros((own, width), bf16)
-
-    def half_copy(i, part):
-        return remote(
-            part.at[1 - parity], half_in.at[i], half_send.at[i], half_recv.at[i], {"tp": mate}
-        )
-
-    def last_copy(i):
-        return remote(
-            half_out.at[i], last_in.at[i], last_send.at[i], last_recv.at[i], {"tp": far}
-        )
-
-    def middle(i, part):
-        half_copy(i, part).wait_recv()
-        half_out[i] = (part[parity, 1 - level].astype(f32) + half_in[i, 1 - level].astype(f32)).astype(bf16)
-        last_copy(i).start()
+        dense_in[...] = jnp.zeros(dense_in.shape, bf16)
+
+    half_copy = remote(mixer_part.at[1 - parity], half_in, half_send, half_recv, {"tp": mate})
+    last_copy = remote(half_out, last_in, last_send, last_recv, {"tp": far})
 
     lax.fori_loop(0, last_block, project_keys, 0)
     loads[9].wait()
@@ -281,22 +331,32 @@
     lax.fori_loop(0, tokens // WINDOW, project, 0)
 
     norm_into(normed, rows_in, 0, 0, tokens, gain)
-    for i in (11, 12, 13):
+    for i in (11, 12):
         loads[i].wait()
     for r in range(2):
         rows = pl.ds(r * (tokens // 2), tokens // 2)
         gate = jnp.dot(normed[rows, :], sg[...], preferred_element_type=f32)
         up = jnp.dot(normed[rows, :], su[...], preferred_element_type=f32)
         shared_hidden[rows, :] = silu_times(gate, up).astype(bf16)
-    for owner in range(4):
-        for c in range(PIECES):
-            cols = pl.ds(c * piece, piece)
-            shared_part[owner % 2, owner // 2, :, cols] = jnp.dot(
-                shared_hidden[pl.ds(owner * own, own), :], sd[:, cols], preferred_element_type=f32
-            ).astype(bf16)
-    half_copy(1, shared_part).start()
-
-    for i in (10, 14):
+
+    def hid_copy(i, device, origin):
+        return remote(
+            shared_hidden.at[rows_at(device * own, own, own)],
+            shared_all.at[:, rows_at(origin * shared_ff, shared_ff, shared_ff)],
+            hid_send.at[i], hid_recv.at[i], {"tp": device},
+        )
+
+    hid_out = [hid_copy(i, device, t) for i, device in enumerate((mate, far, far_mate))]
+    hid_in = [hid_copy(i, device, device) for i, device in enumerate((mate, far, far_mate))]
+    for copy in hid_out:
+        copy.start()
+    shared_all[:, rows_at(t * shared_ff, shared_ff, shared_ff)] = shared_hidden[rows_at(t * own, own, own), :]
+
+    @pl.when(middle_one == 0)
+    def _():
+        lax.fori_loop(1, ep_count, send_far, 0)
+
+    for i in (10, 13):
         loads[i].wait()
     halo_copy((me + 1) % ep_count).wait_recv()
     count = 2 * pairs
@@ -334,29 +394,75 @@
 
     lax.fori_loop(0, tokens // WINDOW, attend, 0)
     for owner in range(4):
-        for c in range(PIECES):
-            cols = pl.ds(c * piece, piece)
+        for c in range(BLOCKS):
+            cols = pl.ds(c * block, block)
             mixer_part[owner % 2, owner // 2, :, cols] = jnp.dot(
                 attended[pl.ds(owner * own, own), :], wo[:, cols], preferred_element_type=f32
             ).astype(bf16)
-    half_copy(0, mixer_part).start()
-    middle(0, mixer_part)
-    middle(1, shared_part)
-
-    def hidden_block(owner, side):
+    half_copy.start()
+    def dealt_copy(n):
+        target = high * 2 * quarter_size + n
+        return remote(
+            slot_block(mirror_slots, n), slot_block(slots_in, mirror),
+            dealt_send.at[n], slot_recv.at[(target - mirror + ep_count) % ep_count], {"ep": target},
+        )
+
+    my_place = (quarter % 2) * quarter_size + seat
+
+    @pl.when(middle_one == 1)
+    def _():
+        for copy in mirrored:
+            copy.wait_recv()
+        mirror_slot_rows = slots_of(mirror_choice)
+        near_ids = lax.broadcasted_iota(jnp.int32, (own, side_rows), 1) + high * side_rows
+        for k, row in enumerate(mirror_slot_rows):
+            mirror_picks[k] = (near_ids == column_of(row)[:, :1].astype(jnp.int32)).astype(f32).astype(bf16)
+            mirror_weights[k] = column_of(mirror_route[k : k + 1, lanes])
+        rows_copy.wait_recv()
+        side_ids = lax.broadcasted_iota(jnp.int32, (side_rows, own), 0) + high * side_rows
+        spread_side = functools.reduce(jnp.logical_or, [side_ids == row for row in mirror_slot_rows])
+        spread_side = spread_side.astype(f32).astype(bf16)
+        for c in range(BLOCKS):
+            cols = pl.ds(c * block, block)
+            mirror_slots[:, cols] = jnp.dot(
+                spread_side, mirror_rows[:, cols], preferred_element_type=f32
+            ).astype(bf16)
+
+        def deal(n, carry):
+            @pl.when(n != my_place)
+            def _():
+                dealt_copy(n).start()
+
+            return carry
+
+        lax.fori_loop(0, 2 * quarter_size, deal, 0)
+        slots_in[rows_at(mirror * capacity, capacity, capacity), :] = mirror_slots[
+            rows_at(my_place * capacity, capacity, capacity), :
+        ]
+
+    half_copy.wait_recv()
+    half_out[...] = (mixer_part[parity, 1 - level].astype(f32) + half_in[1 - level].astype(f32)).astype(bf16)
+    last_copy.start()
+
+    def hidden_block(owner, side, half):
         rows = rows_at(side * side_rows, side_rows, capacity)
-        gate = jnp.dot(slots_in[rows, :], wg[owner], preferred_element_type=f32)
-        up = jnp.dot(slots_in[rows, :], wu[owner], preferred_element_type=f32)
-        hidden[rows, rows_at(owner * ff, ff, ff)] = silu_times(gate, up).astype(bf16)
-
-    from_far[0].wait_recv()
-    to_pass[0].start()
+        weights = jnp.concatenate([wgu[owner, 2 * half], wgu[owner, 2 * half + 1]], axis=1)
+        both = jnp.dot(slots_in[rows, :], weights, preferred_element_type=f32)
+        hidden[rows, rows_at(owner * ff + half * part, part, part)] = silu_times(
+            both[:, :part], both[:, part:]
+        ).astype(bf16)
+
+    def pass_on(i):
+        from_far[i].wait_recv()
+        to_pass[i].start()
+
+    pass_on(0)
 
     def wait_slots(side):
         def wait_one(k, carry):
             source = (me + ep_count - k) % ep_count
 
-            @pl.when(source // (2 * quarter_size) == side)
+            @pl.when((source // (2 * quarter_size) == side) & (middle_one * (source == mirror) == 0))
             def _():
                 slot_copy(k, me, source).wait_recv()
 
@@ -365,23 +471,34 @@
         lax.fori_loop(1, ep_count, wait_one, 0)
 
     wait_slots(high)
-    for i in (15, 16, 17):
+    for i in range(14, 20 + PIECES):
         loads[i].wait()
-    hidden_block(t, high)
+    for half in range(2):
+        hidden_block(t, high, half)
     for copy in from_mate:
         copy.wait_recv()
-    hidden_block(mate, high)
-    from_far[1].wait_recv()
-    to_pass[1].start()
-    hidden_block(far, high)
-    wait_slots(1 - high)
-    hidden_block(t, 1 - high)
-    hidden_block(mate, 1 - high)
-    hidden_block(far, 1 - high)
+    for half in range(2):
+        hidden_block(mate, high, half)
+    pass_on(1)
+    hidden_block(far, high, 0)
+    pass_on(2)
     for i in (0, 1):
         from_pass[i].wait_recv()
-    hidden_block(far_mate, high)
-    hidden_block(far_mate, 1 - high)
+    hidden_block(far_mate, high, 0)
+    wait_slots(1 - high)
+    for half in range(2):
+        hidden_block(t, 1 - high, half)
+        hidden_block(mate, 1 - high, half)
+    hidden_block(far, 1 - high, 0)
+    hidden_block(far_mate, 1 - high, 0)
+    pass_on(3)
+    for side in range(2):
+        hidden_block(far, side, 1)
+    pass_on(4)
+    for i in (2, 3):
+        from_pass[i].wait_recv()
+    for side in range(2):
+        hidden_block(far_mate, side, 1)
 
     def is_low_middle(q):
         return (q % 2) * (1 - q // 2)
@@ -400,7 +517,7 @@
     def back_copy(k, c, owner, target, block):
         cols = pl.ds(c * piece, piece)
         return remote(
-            slot_block(result, owner).at[:, cols], slot_block(back, block).at[:, cols],
+            slot_block(result.at[c], owner), slot_block(back.at[c], block),
             back_send.at[k, c], back_recv.at[block, c], {"ep": target},
         )
 
@@ -435,7 +552,7 @@
     def dense_copy(c):
         cols = pl.ds(c * piece, piece)
         return remote(
-            dense_out.at[:, cols], dense_in.at[:, cols], dense_send.at[c], dense_recv.at[c], {"ep": mirror}
+            dense_out.at[c], dense_in.at[c], dense_send.at[c], dense_recv.at[c], {"ep": mirror}
         )
 
     def relay(c):
@@ -454,46 +571,81 @@
             total = 0.0
             for k in range(top):
                 total = total + mirror_weights[k][:, :1] * jnp.dot(
-                    mirror_picks[k], back[pl.ds(slots, side_rows), cols], preferred_element_type=f32
+                    mirror_picks[k], back[c, pl.ds(slots, side_rows), :], preferred_element_type=f32
                 )
-            dense_out[:, cols] = total.astype(bf16)
+            dense_out[c] = total.astype(bf16)
             dense_copy(c).start()
-
-    for copy in mirrored:
-        copy.wait_recv()
-    near_ids = lax.broadcasted_iota(jnp.int32, (own, side_rows), 1) + high * side_rows
-    for k, row in enumerate(slots_of(mirror_choice)):
-        mirror_picks[k] = (near_ids == column_of(row)[:, :1].astype(jnp.int32)).astype(f32).astype(bf16)
-        mirror_weights[k] = column_of(mirror_route[k : k + 1, lanes])
 
     for c in range(PIECES):
         cols = pl.ds(c * piece, piece)
-        from_far[2 + c].wait_recv()
-        to_pass[2 + c].start()
-        from_pass[2 + c].wait_recv()
-        step = 256
-
-        def down(i, carry, cols=cols):
-            rows = rows_at(i * step, step, step)
-            result[rows, cols] = jnp.dot(
-                hidden[rows, :], wd[:, cols], preferred_element_type=f32
-            ).astype(bf16)
+        from_pass[4 + c].wait_recv()
+        result[c] = jnp.dot(hidden[...], wd[c], preferred_element_type=f32).astype(bf16)
+
+        def keep(owner, block, c=c):
+            back[c, rows_at(block * capacity, capacity, capacity), :] = result[
+                c, rows_at(owner * capacity, capacity, capacity), :
+            ]
+
+        each_back(c, lambda copy: copy.start(), keep)
+        if c + 1 == EARLY:
+            sd_from_far.wait_recv()
+            sd_to_beside.start()
+            sd_passed[0][0].start()
+        if c + 1 < PIECES:
+            pass_on(5 + c)
+        if c >= LAG:
+            relay(c - LAG)
+    for copy in to_far + to_mate + to_pass + hid_out + sd_to_mate:
+        copy.wait_send()
+    for copy in (sd_to_far, sd_to_beside, sd_passed[0][0], half_copy):
+        copy.wait_send()
+
+    @pl.when(middle_one == 1)
+    def _():
+        rows_copy.wait_send()
+        for copy in mirrored:
+            copy.wait_send()
+
+        def dealt_done(n, carry):
+            @pl.when(n != my_place)
+            def _():
+                dealt_copy(n).wait_send()
+
             return carry
 
-        lax.fori_loop(0, slots // step, down, 0)
-
-        def keep(owner, block, cols=cols):
-            back[rows_at(block * capacity, capacity, capacity), cols] = result[
-                rows_at(owner * capacity, capacity, capacity), cols
-            ]
-
-        each_back(c, lambda copy: copy.start(), keep)
-        if c > 0:
-            relay(c - 1)
-    relay(PIECES - 1)
-
-    def summed(i, part):
-        return part[parity, level].astype(f32) + half_in[i, level].astype(f32) + last_in[i].astype(f32)
+        lax.fori_loop(0, 2 * quarter_size, dealt_done, 0)
+
+    halo_copy((me + 1) % ep_count).wait_send()
+
+    def drain(k, carry):
+        target = (me + k) % ep_count
+        other = target // (2 * quarter_size)
+
+        @pl.when(middle_one * (other + high - 2 * other * high) == 0)
+        def _():
+            slot_copy(k, target, me).wait_send()
+
+        return carry
+
+    lax.fori_loop(1, ep_count, drain, 0)
+
+    def back_done(c):
+        each_back(c, lambda copy: copy.wait_send(), None)
+
+        @pl.when(middle_one == 1)
+        def _():
+            dense_copy(c).wait_send()
+
+    sd_from_beside.wait_recv()
+    sd_passed[1][0].start()
+    for c in range(PIECES - LAG, PIECES):
+        relay(c)
+    for copy in hid_in + sd_from_mate + [sd_passed[0][1]]:
+        copy.wait_recv()
+    sd_passed[1][1].wait_recv()
+    for c in range(BLOCKS):
+        cols = pl.ds(c * block, block)
+        expert_sum[:, cols] = jnp.dot(shared_all[...], sd[c // (BLOCKS // 2), :, pl.ds(c % (BLOCKS // 2) * block, block)], preferred_element_type=f32)
 
     for c in range(PIECES):
         cols = pl.ds(c * piece, piece)
@@ -513,42 +665,21 @@
         def _(c=c):
             dense_copy(c).wait_recv()
 
-        total = (
-            shared_part[parity, level, :, cols].astype(f32)
-            + half_in[1, level, :, cols].astype(f32)
-            + dense_in[:, cols].astype(f32)
-        )
+        total = expert_sum[:, cols] + dense_in[c].astype(f32)
         for k in range(top):
             total = total + weights_col[k][:, :1] * jnp.dot(
-                picks[k], back[pl.ds(0, slots), cols], preferred_element_type=f32
+                picks[k], back[c, pl.ds(0, slots), :], preferred_element_type=f32
             )
-        expert_sum[:, cols] = total
-    last_copy(0).wait_recv()
-    mixer_out[...] = summed(0, mixer_part)
-    last_copy(1).wait_recv()
-    expert_out[...] = expert_sum[...] + last_in[1].astype(f32)
-
-    for copy in to_far + to_mate + to_pass:
-        copy.wait_send()
-    for i, part in enumerate((mixer_part, shared_part)):
-        half_copy(i, part).wait_send()
-        last_copy(i).wait_send()
-
-    halo_copy((me + 1) % ep_count).wait_send()
-
-    def drain(k, carry):
-        slot_copy(k, (me + k) % ep_count, me).wait_send()
-        return carry
-
-    lax.fori_loop(1, ep_count, drain, 0)
-    for copy in mirrored:
-        copy.wait_send()
-    for c in range(PIECES):
-        each_back(c, lambda copy: copy.wait_send(), None)
-
-        @pl.when(middle_one == 1)
-        def _(c=c):
-            dense_copy(c).wait_send()
+        expert_out[:, cols] = total
+        if c >= LAG:
+            back_done(c - LAG)
+    last_copy.wait_recv()
+    mixer_out[...] = mixer_part[parity, level].astype(f32) + half_in[level].astype(f32) + last_in[...].astype(f32)
+
+    sd_passed[1][0].wait_send()
+    last_copy.wait_send()
+    for c in range(PIECES - LAG, PIECES):
+        back_done(c)
 
 
 def local(
@@ -588,71 +719,77 @@
     vmem_spec = pl.BlockSpec(memory_space=pltpu.VMEM)
     dma = pltpu.SemaphoreType.DMA
     vmem = pltpu.VMEM
-    count = 2 + PIECES
+    piece = width // PIECES
+    count = 4 + PIECES
+    scratch = [
+        vmem((tokens, width), bf16),
+        vmem((tokens, width), bf16),
+        vmem((1, width), f32),
+        vmem((top, tokens), jnp.int32),
+        vmem((top, tokens), f32),
+        vmem((tp_count, 4, width, ff // 2), bf16),
+        vmem((PIECES, tp_count * ff, piece), bf16),
+        vmem((width, shared_ff), bf16),
+        vmem((width, shared_ff), bf16),
+        vmem((2, tp_count * shared_ff, width // 2), bf16),
+        vmem((tokens, width), bf16),
+        vmem((1, width), f32),
+        vmem(query_weight.shape, bf16),
+        vmem((HEAD_DIM, width), bf16),
+        vmem((HEAD_DIM, width), bf16),
+        vmem(output_weight.shape, bf16),
+        vmem((1, heads), f32),
+        vmem((heads * WINDOW, 2 * HEAD_DIM), f32),
+        vmem((1, 2 * HEAD_DIM), f32),
+        vmem((tokens, 2 * HEAD_DIM), f32),
+        vmem((tokens, 2 * HEAD_DIM), f32),
+        vmem((tokens, heads * HEAD_DIM), bf16),
+        vmem((2, WINDOW + tokens, 2 * HEAD_DIM), bf16),
+        vmem((tokens, heads * HEAD_DIM), bf16),
+        vmem((own, width), bf16),
+        vmem((slots, width), bf16),
+        vmem((slots, width), bf16),
+        vmem((slots, tp_count * ff), bf16),
+        vmem((PIECES, slots, piece), bf16),
+        vmem((PIECES, slots + side_rows, piece), bf16),
+        vmem((top, own, slots), bf16),
+        vmem((top, own, own), f32),
+        vmem((top, tokens), jnp.int32),
+        vmem((top, tokens), f32),
+        vmem((top, own, side_rows), bf16),
+        vmem((top, own, own), f32),
+        vmem((PIECES, own, piece), bf16),
+        vmem((PIECES, own, piece), bf16),
+        vmem((own, width), f32),
+        vmem((2, 2, own, width), bf16),
+        vmem((tokens, shared_ff), bf16),
+        vmem((own, tp_count * shared_ff), bf16),
+        vmem((2, own, width), bf16),
+        vmem((own, width), bf16),
+        vmem((own, width), bf16),
+        vmem((own, width), bf16),
+        vmem((side_rows, width), bf16),
+        dma((20 + PIECES,)),
+        dma((count,)), dma((count,)),
+        dma((count,)), dma((count,)),
+        dma((count,)), dma((count,)),
+        dma((ep_count,)), dma((ep_count,)),
+        dma((ep_count, PIECES)), dma((ep_count + ep_count // 2, PIECES)),
+        dma, dma,
+        dma, dma,
+        dma, dma,
+        dma((2,)), dma((2,)),
+        dma((PIECES,)), dma((PIECES,)),
+        dma((ep_count // 2,)), dma, dma,
+        dma((3,)), dma((3,)),
+        dma((6,)), dma((6,)),
+    ]
     sums = pl.pallas_call(
         functools.partial(mixture_kernel, capacity),
         out_shape=(jax.ShapeDtypeStruct((own, width), f32),) * 2,
         in_specs=[hbm_spec] * 18,
         out_specs=(vmem_spec,) * 2,
-        scratch_shapes=[
-            vmem((tokens, width), bf16),
-            vmem((tokens, width), bf16),
-            vmem((1, width), f32),
-            vmem((top, tokens), jnp.int32),
-            vmem((top, tokens), f32),
-            vmem((tp_count, width, ff), bf16),
-            vmem((tp_count, width, ff), bf16),
-            vmem((tp_count * ff, width), bf16),
-            vmem((width, shared_ff), bf16),
-            vmem((width, shared_ff), bf16),
-            vmem((shared_ff, width), bf16),
-            vmem((tokens, width), bf16),
-            vmem((1, width), f32),
-            vmem(query_weight.shape, bf16),
-            vmem((HEAD_DIM, width), bf16),
-            vmem((HEAD_DIM, width), bf16),
-            vmem(output_weight.shape, bf16),
-            vmem((1, heads), f32),
-            vmem((heads * WINDOW, 2 * HEAD_DIM), f32),
-            vmem((1, 2 * HEAD_DIM), f32),
-            vmem((tokens, 2 * HEAD_DIM), f32),
-            vmem((tokens, 2 * HEAD_DIM), f32),
-            vmem((tokens, heads * HEAD_DIM), bf16),
-            vmem((2, WINDOW + tokens, 2 * HEAD_DIM), bf16),
-            vmem((tokens, heads * HEAD_DIM), bf16),
-            vmem((own, width), bf16),
-            vmem((slots, width), bf16),
-            vmem((slots, width), bf16),
-            vmem((slots, tp_count * ff), bf16),
-            vmem((slots, width), bf16),
-            vmem((slots + side_rows, width), bf16),
-            vmem((top, own, slots), bf16),
-            vmem((top, own, own), f32),
-            vmem((top, tokens), jnp.int32),
-            vmem((top, tokens), f32),
-            vmem((top, own, side_rows), bf16),
-            vmem((top, own, own), f32),
-            vmem((own, width), bf16),
-            vmem((own, width), bf16),
-            vmem((own, width), f32),
-            vmem((2, 2, own, width), bf16),
-            vmem((2, 2, own, width), bf16),
-            vmem((tokens, shared_ff), bf16),
-            vmem((2, 2, own, width), bf16),
-            vmem((2, own, width), bf16),
-            vmem((2, own, width), bf16),
-            dma((18,)),
-            dma((count,)), dma((count,)),
-            dma((count,)), dma((count,)),
-            dma((count,)), dma((count,)),
-            dma((ep_count,)), dma((ep_count,)),
-            dma((ep_count, PIECES)), dma((ep_count + ep_count // 2, PIECES)),
-            dma((2,)), dma((2,)),
-            dma((2,)), dma((2,)),
-            dma, dma,
-            dma((2,)), dma((2,)),
-            dma((PIECES,)), dma((PIECES,)),
-        ],
+        scratch_shapes=scratch,
         compiler_params=pltpu.CompilerParams(
             collective_id=0, has_side_effects=True, vmem_limit_bytes=62 * 1024 * 1024
         ),
@@ -662,7 +799,17 @@
         mixer_input, gain_mixer[None, :], query_weight, key_weight.T, value_weight.T, output_weight,
         sink_logits[None, :], frequencies(HEAD_DIM),
     )
-    return tuple(value.astype(bf16) for value in sums)
+    def round_both(a_ref, b_ref, mixer_out, expert_out):
+        mixer_out[...] = a_ref[...].astype(bf16)
+        expert_out[...] = b_ref[...].astype(bf16)
+
+    return pl.pallas_call(
+        round_both,
+        grid=(1,),
+        out_shape=(jax.ShapeDtypeStruct((own, width), bf16),) * 2,
+        in_specs=(pl.BlockSpec((own, width), lambda i: (i, 0)),) * 2,
+        out_specs=(pl.BlockSpec((own, width), lambda i: (i, 0)),) * 2,
+    )(*sums)
 
 
 def solution(mesh):

time: 105 us -> 103 us (0.981); the launches traced: 103 us -> 103 us
  other arithmetic: 3.03 us -> 0 us
  Pallas kernels: 99.7 us -> 102 us
    convert_element_type x2 -> x0, other arithmetic: 3.03 us -> none  [local(): return tuple((value.astype(bf16) for value in sums))]
    pallas_call x0 -> x1, Pallas kernels: none -> 2.56 us  [local(): pl.pallas_call(round_both, grid=(1,), out_shape=(jax.ShapeDtypeStruct((ow...]
where the time goes in v2:
time: 103 us
  Pallas kernels  102 us (99%)
    pallas_call x1, Pallas kernels, local(): pl.pallas_call(functools.partial(mixture_kernel, capacity), out_shape=(ja...  99.5 us
    pallas_call x1, Pallas kernels, local(): pl.pallas_call(round_both, grid=(1,), out_shape=(jax.ShapeDtypeStruct((ow...  2.56 us

profile of v2, /device:TPU:9, one launch (start us, length us, event | category | flops | bytes accessed | tf_op | source)
XLA Modules:
  0.0 102.7 jit_solution(3897861476810204544)
XLA Ops:
  0.6 99.5 %shard_map.185 = (f32[128,2048]{1,0:T(8,128)}, f32[128,2048]{1,0:T(8,128)}) custom-call(bf16[512,2048]{1,0:T(8,128)(2,1)} %x_ref.1, f32[1,2048]{1,0:T(1,128)} %bitcast.15, s32[2,512]{1,0:T(2,128)} %bitcast.17, f32[2,512]{1,0:T(2,128)} %bitcast.18, bf16[2048,256]{1,0:T(8,128)(2,1)} %bitcast.10, bf16[2048,256]{1,0:T(8,128)(2,1)} %bitcast.11, ...), custom_call_target="tpu_custom_call" | custom-call | tf_op jit(solution)/shard_map/pallas_call | solution.py:787
  100.2 2.6 %shard_map.186 = (bf16[128,2048]{1,0:T(8,128)(2,1)}, bf16[128,2048]{1,0:T(8,128)(2,1)}) custom-call(f32[128,2048]{1,0:T(8,128)} %get-tuple-element.4.a_ref, f32[128,2048]{1,0:T(8,128)} %get-tuple-element.5.b_ref), custom_call_target="tpu_custom_call" | custom-call | tf_op jit(solution)/shard_map/pallas_call | solution.py:806

commit v3 on v2

--- a/solution.py
+++ b/solution.py
@@ -53,11 +53,11 @@
     x_ref, gain_ref, choice_ref, route_ref,
     wg_ref, wu_ref, wd_ref, sg_ref, su_ref, sd_ref,
     mx_ref, mgain_ref, wq_ref, wk_ref, wv_ref, wo_ref, sink_ref, freq_ref,
-    mixer_out, expert_out,
+    mixer_ref, expert_ref,
     rows_in, normed, gain, choice, route, wgu, wd, sg, su, sd,
     mixer_in, mixer_gain, wq, wk, wv, wo, sink, sunk, freq, cosines, sines, queries, band, attended,
     own_rows, slots_out, slots_in, hidden, result, back, picks, weights_col,
-    mirror_choice, mirror_route, mirror_picks, mirror_weights, dense_out, dense_in, expert_sum,
+    mirror_choice, mirror_route, mirror_picks, mirror_weights, dense_out, dense_in, expert_sum, mixer_out, expert_out, out_sem,
     mixer_part, shared_hidden, shared_all, half_in, half_out, last_in, mirror_rows, mirror_slots,
     load_sem, far_send, far_recv, mate_send, mate_recv, pass_send, pass_recv,
     slot_send, slot_recv, back_send, back_recv, half_send, half_recv, last_send, last_recv,
@@ -647,6 +647,13 @@
         cols = pl.ds(c * block, block)
         expert_sum[:, cols] = jnp.dot(shared_all[...], sd[c // (BLOCKS // 2), :, pl.ds(c % (BLOCKS // 2) * block, block)], preferred_element_type=f32)
 
+    mixer_copy = pltpu.make_async_copy(mixer_out, mixer_ref, out_sem.at[PIECES])
+
+    def expert_copy(c):
+        return pltpu.make_async_copy(
+            expert_out.at[c], expert_ref.at[:, pl.ds(c * piece, piece)], out_sem.at[c]
+        )
+
     for c in range(PIECES):
         cols = pl.ds(c * piece, piece)
 
@@ -670,16 +677,23 @@
             total = total + weights_col[k][:, :1] * jnp.dot(
                 picks[k], back[c, pl.ds(0, slots), :], preferred_element_type=f32
             )
-        expert_out[:, cols] = total
+        expert_out[c] = total.astype(bf16)
+        expert_copy(c).start()
+        if c == PIECES - 2:
+            last_copy.wait_recv()
+            mixer_sum = mixer_part[parity, level].astype(f32) + half_in[level].astype(f32)
+            mixer_out[...] = (mixer_sum + last_in[...].astype(f32)).astype(bf16)
+            mixer_copy.start()
         if c >= LAG:
             back_done(c - LAG)
-    last_copy.wait_recv()
-    mixer_out[...] = mixer_part[parity, level].astype(f32) + half_in[level].astype(f32) + last_in[...].astype(f32)
 
     sd_passed[1][0].wait_send()
     last_copy.wait_send()
     for c in range(PIECES - LAG, PIECES):
         back_done(c)
+    mixer_copy.wait()
+    for c in range(PIECES):
+        expert_copy(c).wait()
 
 
 def local(
@@ -716,7 +730,6 @@
     heads = query_weight.shape[1] // HEAD_DIM
     assert heads % 2 == 0 and key_weight.shape[1] == HEAD_DIM and own % WINDOW == 0
     hbm_spec = pl.BlockSpec(memory_space=pltpu.HBM)
-    vmem_spec = pl.BlockSpec(memory_space=pltpu.VMEM)
     dma = pltpu.SemaphoreType.DMA
     vmem = pltpu.VMEM
     piece = width // PIECES
@@ -761,6 +774,9 @@
         vmem((PIECES, own, piece), bf16),
         vmem((PIECES, own, piece), bf16),
         vmem((own, width), f32),
+        vmem((own, width), bf16),
+        vmem((PIECES, own, piece), bf16),
+        dma((1 + PIECES,)),
         vmem((2, 2, own, width), bf16),
         vmem((tokens, shared_ff), bf16),
         vmem((own, tp_count * shared_ff), bf16),
@@ -786,9 +802,9 @@
     ]
     sums = pl.pallas_call(
         functools.partial(mixture_kernel, capacity),
-        out_shape=(jax.ShapeDtypeStruct((own, width), f32),) * 2,
+        out_shape=(jax.ShapeDtypeStruct((own, width), bf16),) * 2,
         in_specs=[hbm_spec] * 18,
-        out_specs=(vmem_spec,) * 2,
+        out_specs=(hbm_spec,) * 2,
         scratch_shapes=scratch,
         compiler_params=pltpu.CompilerParams(
             collective_id=0, has_side_effects=True, vmem_limit_bytes=62 * 1024 * 1024
@@ -800,8 +816,8 @@
         sink_logits[None, :], frequencies(HEAD_DIM),
     )
     def round_both(a_ref, b_ref, mixer_out, expert_out):
-        mixer_out[...] = a_ref[...].astype(bf16)
-        expert_out[...] = b_ref[...].astype(bf16)
+        mixer_out[...] = a_ref[...]
+        expert_out[...] = b_ref[...]
 
     return pl.pallas_call(
         round_both,

time: 103 us -> 102 us (level)
  no operation moved by 1% of the time
where the time goes in v3:
time: 102 us; the launch traced here: 101 us
  Pallas kernels  101 us (99%)
    pallas_call x1, Pallas kernels, local(): pl.pallas_call(functools.partial(mixture_kernel, capacity), out_shape=(ja...  98.6 us
    pallas_call x1, Pallas kernels, local(): pl.pallas_call(round_both, grid=(1,), out_shape=(jax.ShapeDtypeStruct((ow...  2.2 us

profile of v3, /device:TPU:9, one launch (start us, length us, event | category | flops | bytes accessed | tf_op | source)
XLA Modules:
  0.0 101.4 jit_solution(8591045795543268259)
XLA Ops:
  0.6 98.6 %shard_map.185 = (bf16[128,2048]{1,0:T(8,128)(2,1)}, bf16[128,2048]{1,0:T(8,128)(2,1)}) custom-call(bf16[512,2048]{1,0:T(8,128)(2,1)} %x_ref.1, f32[1,2048]{1,0:T(1,128)} %bitcast.15, s32[2,512]{1,0:T(2,128)} %bitcast.17, f32[2,512]{1,0:T(2,128)} %bitcast.18, bf16[2048,256]{1,0:T(8,128)(2,1)} %bitcast.10, bf16[2048,256]{1,0:T(8,128)(2,1)} %bitcast.11, ...), custom_call_target="tpu_custom_call" | custom-call | tf_op jit(solution)/shard_map/pallas_call | solution.py:803
  99.2 2.2 %shard_map.186 = (bf16[128,2048]{1,0:T(8,128)(2,1)}, bf16[128,2048]{1,0:T(8,128)(2,1)}) custom-call(bf16[128,2048]{1,0:T(8,128)(2,1)} %get-tuple-element.4.a_ref, bf16[128,2048]{1,0:T(8,128)(2,1)} %get-tuple-element.5.b_ref), custom_call_target="tpu_custom_call" | custom-call | tf_op jit(solution)/shard_map/pallas_call | solution.py:822

commit v4 on v3

--- a/solution.py
+++ b/solution.py
@@ -485,13 +485,13 @@
     for i in (0, 1):
         from_pass[i].wait_recv()
     hidden_block(far_mate, high, 0)
+    pass_on(3)
     wait_slots(1 - high)
     for half in range(2):
         hidden_block(t, 1 - high, half)
         hidden_block(mate, 1 - high, half)
     hidden_block(far, 1 - high, 0)
     hidden_block(far_mate, 1 - high, 0)
-    pass_on(3)
     for side in range(2):
         hidden_block(far, side, 1)
     pass_on(4)

time: 102 us -> 102 us (level)
  no operation moved by 1% of the time
where the time goes in v4:
time: 102 us; the launch traced here: 101 us
  Pallas kernels  101 us (99%)
    pallas_call x1, Pallas kernels, local(): pl.pallas_call(functools.partial(mixture_kernel, capacity), out_shape=(ja...  98.6 us
    pallas_call x1, Pallas kernels, local(): pl.pallas_call(round_both, grid=(1,), out_shape=(jax.ShapeDtypeStruct((ow...  2.2 us

profile of v4, /device:TPU:9, one launch (start us, length us, event | category | flops | bytes accessed | tf_op | source)
XLA Modules:
  0.0 101.4 jit_solution(17521756084649577595)
XLA Ops:
  0.6 98.6 %shard_map.185 = (bf16[128,2048]{1,0:T(8,128)(2,1)}, bf16[128,2048]{1,0:T(8,128)(2,1)}) custom-call(bf16[512,2048]{1,0:T(8,128)(2,1)} %x_ref.1, f32[1,2048]{1,0:T(1,128)} %bitcast.15, s32[2,512]{1,0:T(2,128)} %bitcast.17, f32[2,512]{1,0:T(2,128)} %bitcast.18, bf16[2048,256]{1,0:T(8,128)(2,1)} %bitcast.10, bf16[2048,256]{1,0:T(8,128)(2,1)} %bitcast.11, ...), custom_call_target="tpu_custom_call" | custom-call | tf_op jit(solution)/shard_map/pallas_call | solution.py:803
  99.2 2.2 %shard_map.186 = (bf16[128,2048]{1,0:T(8,128)(2,1)}, bf16[128,2048]{1,0:T(8,128)(2,1)}) custom-call(bf16[128,2048]{1,0:T(8,128)(2,1)} %get-tuple-element.4.a_ref, bf16[128,2048]{1,0:T(8,128)(2,1)} %get-tuple-element.5.b_ref), custom_call_target="tpu_custom_call" | custom-call | tf_op jit(solution)/shard_map/pallas_call | solution.py:822
